TPU v7x, 128 devices: a whole 4x4x4 slice. The times are simulated.
128 devices in a mesh: ep: 64 (over z, y, x), tp: 2 (over core).
Axes of the slice: x: 4, y: 4, z: 4, core: 2. Of those that a mesh axis runs over, the one named last changes fastest.
Arguments:
- tokens: bfloat16 [24576, 3072], P('ep', 'tp'), may hold values from -6 to 6
- cotangent: bfloat16 [24576, 3072], P('ep', 'tp'), may hold values from -6 to 6
- experts: int32 [24576, 2], P('ep'), may hold values from 0 to 63, all different within a row; in each aligned block of 384 rows (0 to 383, 384 to 767, ...) at most 18 rows name the same one
- gate: float32 [24576, 2], P('ep'), may hold values from 0.2 to 1
- w_gate: bfloat16 [64, 3072, 768], P('ep', None, 'tp'), may hold values from -0.109375 to 0.109375
- w_up: bfloat16 [64, 3072, 768], P('ep', None, 'tp'), may hold values from -0.109375 to 0.109375
- w_down: bfloat16 [64, 768, 3072], P('ep', 'tp'), may hold values from -0.21875 to 0.21875
Outputs:
- token_grad: bfloat16 [24576, 3072], P('ep', 'tp')
- gate_grad: float32 [24576, 2], P('ep')
- gate_weight_grad: bfloat16 [64, 3072, 768], P('ep', None, 'tp')
- up_weight_grad: bfloat16 [64, 3072, 768], P('ep', None, 'tp')
- down_weight_grad: bfloat16 [64, 768, 3072], P('ep', 'tp')
- gate_row_norms: float32 [64, 3072], P('ep')
- up_row_norms: float32 [64, 3072], P('ep')
- down_row_norms: float32 [64, 768], P('ep', 'tp')
Inputs may be any that keep to these rules, and one draw needn't show every extreme that they name: A row names 2 different experts. In each aligned block of 384 rows (the rows of one index of ep) no expert is named by more than 18 rows, a bound that some block reaches.
All inputs are finite; a program needn't handle non-finite values.
Results may differ from a plain program's by a relative error of at most 0.008.
Values may be sent and summed in bfloat16 or wider, within the bound.
No kernel may reach another device: no remote copies, remote signals or barrier semaphores. Data moves between devices by JAX's collectives and lax.ppermute only.
A program may use at most 128 MiB of HBM per device.

v0:
```python
import functools

import jax
import jax.numpy as jnp
from jax import lax
from jax.experimental import pallas as pl
from jax.experimental.pallas import tpu as pltpu
from jax.sharding import PartitionSpec as P


E = 64
TOK = 384
H = 1536
Q = 384
F1 = E * 8
BF = jnp.bfloat16
F32 = jnp.float32


def iota(shape, axis):
    return lax.broadcasted_iota(jnp.int32, shape, axis)


def dot(a, b):
    return lax.dot_general(a, b, (((1,), (0,)), ((), ())), preferred_element_type=F32)


def dot_last(a, b):
    return lax.dot_general(a, b, (((1,), (1,)), ((), ())), preferred_element_type=F32)


def dot_rows(a, b):
    return lax.dot_general(a, b, (((0,), (0,)), ((), ())), preferred_element_type=F32)


def ones_where(mask):
    return jnp.where(mask, 1.0, 0.0)


def named_by(exp):
    ids = iota((E, TOK), 0)
    return exp[0:1, :] == ids, exp[1:2, :] == ids


def slot_ranks(exp):
    first, second = named_by(exp)
    named = ones_where(first) + ones_where(second)
    earlier = ones_where(iota((TOK, TOK), 0) < iota((TOK, TOK), 1)).astype(BF)
    return named, dot(named.astype(BF), earlier)


def spread_rows(per_expert):
    spread = ones_where(iota((F1, E), 0) // 8 == iota((F1, E), 1)).astype(BF)
    return dot(spread, per_expert)


def row_slots(piece):
    i = iota((F1, TOK), 0) % 8
    return jnp.where(piece == 2, 16 + i % 2, i + 8 * piece).astype(F32)


def put_last(rows):
    row = iota((F1, 128), 0)
    col = iota((F1, 128), 1)
    total = jnp.zeros((F1, Q), F32)
    for q in range(4):
        place = ones_where(row == col // 2 * 8 + 2 * q + col % 2).astype(BF)
        total = total + dot(place, rows[:, q * Q : (q + 1) * Q])
    return total


def send_tokens_kernel(exp_ref, gate_ref, src_ref, out_ref, ranks_ref, gates_ref, small_ref):
    b = pl.program_id(0)

    @pl.when(b == 0)
    def _():
        exp = exp_ref[...]
        named, ranks = slot_ranks(exp)
        small = jnp.where(named > 0.5, ranks, -1.0).astype(BF)
        small_ref[...] = small
        ranks_ref[...] = spread_rows(small)

    def rows(piece, lo, hi):
        hit = ones_where(ranks_ref[...] == row_slots(jnp.int32(piece))).astype(BF)
        return dot(hit, src_ref[:, lo:hi]).reshape(E, 8, hi - lo).astype(BF)

    @pl.when(b == 0)
    def _():
        out_ref[...] = rows(0, 0, 1152)

    @pl.when(b == 1)
    def _():
        out_ref[:, :, 0:384] = rows(0, 1152, 1536)
        out_ref[:, :, 384:1152] = rows(1, 0, 768)

    @pl.when(b == 2)
    def _():
        out_ref[:, :, 0:768] = rows(1, 768, 1536)
        row = iota((128, E), 0)
        spread = ones_where(row // 2 == iota((128, E), 1)).astype(BF)
        slot = (16 + iota((128, TOK), 0) % 2).astype(F32)
        hit = ones_where(dot(spread, small_ref[...]) == slot).astype(BF)
        last = dot(hit, src_ref[...]).astype(BF)
        out_ref[:, :, 768:1152] = put_last(last).reshape(E, 8, Q).astype(BF)
        first, second = named_by(exp_ref[...])
        gate = gate_ref[...]
        rest = jnp.where(first, gate[0:1, :], 0.0) + jnp.where(second, gate[1:2, :], 0.0)
        total = jnp.zeros((F1, TOK), F32)
        for _ in range(3):
            part = rest.astype(BF)
            rest = rest - part.astype(F32)
            total = total + spread_rows(part)
        gates_ref[...] = total


def send_tokens(exp_t, gate_t, tokens):
    small = pl.BlockSpec((2, TOK), lambda b: (0, 0))
    table = pl.BlockSpec((F1, TOK), lambda b: (0, 0))
    shape = jax.ShapeDtypeStruct((F1, TOK), F32)
    return pl.pallas_call(
        send_tokens_kernel,
        grid=(3,),
        in_specs=[small, small, pl.BlockSpec((TOK, H), lambda b: (0, 0))],
        out_specs=[pl.BlockSpec((E, 8, 1152), lambda b: (0, 0, b)), table, table],
        out_shape=[jax.ShapeDtypeStruct((E, 8, 3456), BF), shape, shape],
        scratch_shapes=[pltpu.VMEM((E, TOK), BF)],
        name="send_tokens",
    )(exp_t, gate_t, tokens)


def send_kernel(lo, last, ranks_ref, gates_ref, src_ref, out_ref):
    b = pl.program_id(0) + lo

    def scaled(hit, rows):
        rows = rows * jnp.sum(jnp.where(hit, gates_ref[...], 0.0), axis=1, keepdims=True)
        return rows.reshape(E, 8, Q).astype(BF)

    @pl.when(b < 8)
    def _():
        hit = ranks_ref[...] == row_slots(b // 4)
        src = src_ref[:, pl.ds(pl.multiple_of((b % 4) * Q, Q), Q)]
        out_ref[...] = scaled(hit, dot(ones_where(hit).astype(BF), src))

    if last:

        @pl.when(b == 8)
        def _():
            hit = ranks_ref[...] == row_slots(jnp.int32(2))
            block = (iota((F1, TOK), 0) % 8) // 2
            total = jnp.zeros((F1, Q), F32)
            for q in range(4):
                pick = ones_where(hit & (block == q)).astype(BF)
                total = total + dot(pick, src_ref[:, q * Q : (q + 1) * Q])
            out_ref[...] = scaled(hit, total)


def send(ranks, gates, src, lo, hi):
    whole = pl.BlockSpec((F1, TOK), lambda b: (0, 0))
    return pl.pallas_call(
        functools.partial(send_kernel, lo, hi == 9),
        grid=(hi - lo,),
        in_specs=[whole, whole, pl.BlockSpec((TOK, H), lambda b: (0, 0))],
        out_specs=pl.BlockSpec((E, 8, Q), lambda b: (0, 0, b)),
        out_shape=jax.ShapeDtypeStruct((E, 8, (hi - lo) * Q), BF),
        name="send",
    )(ranks, gates, src)


def unpack_last(last):
    flat = last.astype(F32).reshape(F1, Q).astype(BF)
    row = iota((128, F1), 0)
    pieces = []
    for q in range(4):
        pick = ones_where(row // 2 * 8 + 2 * q + row % 2 == iota((128, F1), 1)).astype(BF)
        pieces.append(dot(pick, flat).astype(BF))
    return pieces


def unpack_kernel(steps, core_ref, own_ref, other_ref, own_last_ref, other_last_ref, out_ref):
    b = pl.program_id(0)
    core = core_ref[0]
    sides = ((core, own_ref, own_last_ref), (1 - core, other_ref, other_last_ref))

    @pl.when(b < steps)
    def _():
        for half, rows_ref, _ in sides:
            rows = rows_ref[...].astype(F32).reshape(128, H).astype(BF)
            out_ref[:, pl.ds(pl.multiple_of(half * H, H), H)] = rows

    @pl.when(b == steps)
    def _():
        for half, _, last_ref in sides:
            for q, piece in enumerate(unpack_last(last_ref[...])):
                out_ref[:, pl.ds(pl.multiple_of(half * H + q * Q, Q), Q)] = piece


def unpack(core, own, other):
    wide = (own.shape[2] - Q) // H
    steps = 4 * wide

    def rows_at(b):
        bb = jnp.minimum(b, steps - 1)
        return (bb % 4, 0, bb // 4)

    rows = pl.BlockSpec((16, 8, H), rows_at)
    last = pl.BlockSpec((E, 8, Q), lambda b: (0, 0, wide * 4))
    return pl.pallas_call(
        functools.partial(unpack_kernel, steps),
        grid=(steps + 1,),
        in_specs=[pl.BlockSpec(memory_space=pltpu.SMEM), rows, rows, last, last],
        out_specs=pl.BlockSpec((128, 2 * H), lambda b: (b, 0)),
        out_shape=jax.ShapeDtypeStruct((steps * 128 + 128, 2 * H), BF),
        name="unpack",
    )(core, own, other, own, other)


def pack_kernel(mine_ref, got_ref, mine_last_ref, got_last_ref, part_ref, got_part_ref, out_ref):
    b = pl.program_id(0)

    @pl.when(b < 3)
    def _():
        total = mine_ref[...].astype(F32) + got_ref[...].astype(F32)
        out_ref[...] = total.reshape(E, 8, 512).astype(BF)

    @pl.when(b == 3)
    def _():
        total = (mine_last_ref[...].astype(F32) + got_last_ref[...].astype(F32)).astype(BF)
        out_ref[:, :, 0:Q] = put_last(total).reshape(E, 8, Q).astype(BF)
        products = (part_ref[...] + got_part_ref[...]).astype(BF).astype(F32)
        at = iota((E, 1152), 1)
        source = jnp.where(at < 1024, at % 512 // 8, (at - 1024) // 2)
        mine = jnp.where(source == iota((E, 1152), 0), products, 0.0).astype(BF)
        at = iota((1152, 128), 0)
        slot = jnp.where(at < 1024, at // 512 * 8 + at % 8, 16 + at % 2)
        table = dot(mine, ones_where(slot == iota((1152, 128), 1)).astype(BF)).astype(BF)
        place = ones_where(iota((F1, E), 0) == 8 * iota((F1, E), 1)).astype(BF)
        out_ref[:, :, Q:512] = dot(place, table).reshape(E, 8, 128).astype(BF)


def pack(mine, got, part, got_part):
    main = pl.BlockSpec((F1, 512), lambda b: (0, jnp.minimum(b, 2)))
    last = pl.BlockSpec((128, H), lambda b: (4, 0))
    line = pl.BlockSpec((1, 1152), lambda b: (0, 0))
    return pl.pallas_call(
        pack_kernel,
        grid=(4,),
        in_specs=[main, main, last, last, line, line],
        out_specs=pl.BlockSpec((E, 8, 512), lambda b: (0, 0, b)),
        out_shape=jax.ShapeDtypeStruct((E, 8, 2048), BF),
        name="pack",
    )(mine, got, mine, got, part, got_part)


def token_ranks_kernel(exp_ref, out_ref):
    exp = exp_ref[...]
    ids = iota((TOK, E), 1)
    named = ones_where(exp[:, 0:1] == ids) + ones_where(exp[:, 1:2] == ids)
    earlier = ones_where(iota((TOK, TOK), 1) < iota((TOK, TOK), 0)).astype(BF)
    ranks = jnp.where(named > 0.5, dot(earlier, named.astype(BF)), -1.0).astype(BF)
    spread = ones_where(iota((E, F1), 0) == iota((E, F1), 1) // 8).astype(BF)
    out_ref[...] = dot(ranks, spread)


def token_ranks(experts):
    return pl.pallas_call(
        token_ranks_kernel, out_shape=jax.ShapeDtypeStruct((TOK, F1), F32), name="token_ranks"
    )(experts)


def flat_rows(ref):
    return ref[...].astype(F32).reshape(F1, ref.shape[2]).astype(BF)


def column_slots(piece):
    i = iota((TOK, F1), 1) % 8
    return (16 + i % 2 if piece == 2 else i + 8 * piece).astype(F32)


def combine_one_kernel(ranks_ref, one_ref, out_ref):
    hit = ones_where(ranks_ref[...] == column_slots(0)).astype(BF)
    out_ref[...] = dot(hit, flat_rows(one_ref))


def combine_one(ranks, one):
    return pl.pallas_call(
        combine_one_kernel,
        grid=(4,),
        in_specs=[
            pl.BlockSpec((TOK, F1), lambda b: (0, 0)),
            pl.BlockSpec((E, 8, Q), lambda b: (0, 0, b)),
        ],
        out_specs=pl.BlockSpec((TOK, Q), lambda b: (0, b)),
        out_shape=jax.ShapeDtypeStruct((TOK, H), F32),
        name="combine_one",
    )(ranks, one)


def combine_two_kernel(ranks_ref, exp_ref, gate_ref, sum_ref, two_ref, last_ref, prod_ref, out_ref, gate_out_ref):
    b = pl.program_id(0)

    @pl.when(b == 0)
    def _():
        pick = ones_where(iota((E, F1), 1) == 8 * iota((E, F1), 0)).astype(BF)
        table = dot(pick, flat_rows(prod_ref)).astype(BF)
        for k in range(2):
            exp = exp_ref[:, k : k + 1]
            at = iota((TOK, F1), 1) == 8 * exp
            rank = jnp.sum(jnp.where(at, ranks_ref[...], 0.0), axis=1, keepdims=True)
            found = dot(ones_where(iota((TOK, E), 1) == exp).astype(BF), table)
            here = iota((TOK, 128), 1).astype(F32) == rank
            found = jnp.sum(jnp.where(here, found, 0.0), axis=1, keepdims=True)
            gate_out_ref[:, k : k + 1] = found / gate_ref[:, k : k + 1]

    ranks = ranks_ref[...]
    block = iota((TOK, F1), 1) % 8 // 2
    total = sum_ref[...] + dot(ones_where(ranks == column_slots(1)).astype(BF), flat_rows(two_ref))
    hit = (ranks == column_slots(2)) & (block == b)
    out_ref[...] = (total + dot(ones_where(hit).astype(BF), flat_rows(last_ref))).astype(BF)


def combine_two(ranks, experts, gate, total, two):
    small = pl.BlockSpec((TOK, 2), lambda b: (0, 0))
    return pl.pallas_call(
        combine_two_kernel,
        grid=(4,),
        in_specs=[
            pl.BlockSpec((TOK, F1), lambda b: (0, 0)),
            small,
            small,
            pl.BlockSpec((TOK, Q), lambda b: (0, b)),
            pl.BlockSpec((E, 8, Q), lambda b: (0, 0, b)),
            pl.BlockSpec((E, 8, Q), lambda b: (0, 0, 4)),
            pl.BlockSpec((E, 8, 128), lambda b: (0, 0, 15)),
        ],
        out_specs=[pl.BlockSpec((TOK, Q), lambda b: (0, b)), small],
        out_shape=[jax.ShapeDtypeStruct((TOK, H), BF), jax.ShapeDtypeStruct((TOK, 2), F32)],
        name="combine_two",
    )(ranks, experts, gate, total, two, two, two)


def weight_grads_kernel(x_ref, g1_ref, u1_ref, g2_ref, u2_ref, gate_ref, up_ref, norm_ref, turned_ref):
    @pl.when(pl.program_id(0) == 0)
    def _():
        for at, one_ref, two_ref in ((0, g1_ref, g2_ref), (384, u1_ref, u2_ref)):
            turned_ref[at : at + 384, 0:F1] = one_ref[...].T
            turned_ref[at : at + 384, F1:1152] = two_ref[...].T

    total = dot(turned_ref[...], x_ref[...])
    for k, ref in enumerate((gate_ref, up_ref)):
        part = total[384 * k : 384 * k + 384]
        norm_ref[k : k + 1, :] = jnp.sum(part * part, axis=0, keepdims=True)
        ref[...] = part.T.astype(BF)


def weight_grads(rows, g1, u1, g2, u2):
    def whole(a):
        return pl.BlockSpec(a.shape, lambda b: (0, 0))

    block = pl.BlockSpec((512, 384), lambda b: (b, 0))
    shape = jax.ShapeDtypeStruct((2 * H, 384), BF)
    return pl.pallas_call(
        weight_grads_kernel,
        grid=(6,),
        in_specs=[pl.BlockSpec((1152, 512), lambda b: (0, b)), whole(g1), whole(u1), whole(g2), whole(u2)],
        out_specs=[block, block, pl.BlockSpec((2, 512), lambda b: (0, b))],
        out_shape=[shape, shape, jax.ShapeDtypeStruct((2, 2 * H), F32)],
        scratch_shapes=[pltpu.VMEM((768, 1152), BF)],
        name="weight_grads",
    )(rows, g1, u1, g2, u2)


def to_experts(x):
    return lax.all_to_all(x, "ep", split_axis=0, concat_axis=0, tiled=True)


def swap_cores(x):
    return lax.ppermute(x, "tp", [(0, 1), (1, 0)])


def half(mat, index, axis):
    return lax.dynamic_slice_in_dim(mat, index * H, H, axis)


def step(tokens, cotangent, experts, gate, w_gate, w_up, w_down):
    core = lax.axis_index("tp").astype(jnp.int32)
    core_arg = core.reshape(1)
    gate_mat, up_mat, down_mat = w_gate[0], w_up[0], w_down[0]
    exp_t, gate_t = experts.T, gate.T
    gates = [half(gate_mat, index, 0) for index in (core, 1 - core)]
    ups = [half(up_mat, index, 0) for index in (core, 1 - core)]
    downs = [half(down_mat, index, 1) for index in (core, 1 - core)]
    tok_own, ranks, gates_of = send_tokens(exp_t, gate_t, tokens)
    tok_own = to_experts(tok_own)
    cot_one = send(ranks, gates_of, cotangent, 0, 4)
    cot_one = to_experts(cot_one)
    cot_two = send(ranks, gates_of, cotangent, 4, 9)
    by_token = token_ranks(experts)
    cot_two = to_experts(cot_two)
    tok_other = swap_cores(tok_own)

    rows_in = unpack(core_arg, tok_own, tok_other)
    gate_pre = dot(rows_in, gate_mat)
    up_pre = dot(rows_in, up_mat)
    sigma = jax.nn.sigmoid(gate_pre)
    active = gate_pre * sigma
    hidden = (active * up_pre).astype(BF)
    gate_slope = up_pre * sigma * (1.0 + gate_pre * (1.0 - sigma))

    def chunk(rows, lo, hi):
        grad = rows[0]
        for part in rows[1:]:
            grad = grad + part
        parts = jnp.sum(hidden[lo:hi].astype(F32) * grad, axis=1)
        gate_grad_pre = (grad * gate_slope[lo:hi]).astype(BF)
        up_grad_pre = (grad * active[lo:hi]).astype(BF)

        def partial(index):
            return (dot_last(gate_grad_pre, gates[index]) + dot_last(up_grad_pre, ups[index])).astype(BF)

        sent = swap_cores(partial(1))
        return parts, gate_grad_pre, up_grad_pre, partial(0), sent

    cot_one_other = swap_cores(cot_one)
    own = cot_one.reshape(F1, H)
    other = cot_one_other.reshape(F1, H)
    one = chunk((dot_last(own, downs[0]), dot_last(other, downs[1])), 0, F1)
    back_one = (one[3].astype(F32) + one[4].astype(F32)).astype(BF).reshape(E, 8, H)
    back_one = to_experts(back_one)

    cot_two_other = swap_cores(cot_two)
    rows_two = unpack(core_arg, cot_two, cot_two_other)
    two = chunk((dot_last(rows_two, down_mat),), F1, 1152)
    parts = jnp.concatenate([one[0], two[0]])
    parts = parts.reshape(1, 1152)
    back_two = pack(two[3], two[4], parts, swap_cores(parts))
    back_two = to_experts(back_two)

    down_own = dot_rows(hidden[:F1], own)
    down_other = dot_rows(hidden[:F1], other)
    gate_grad, up_grad, norms = weight_grads(rows_in, one[1], one[2], two[1], two[2])
    norms = norms + swap_cores(norms)
    down_one = jnp.where(
        core == 0,
        jnp.concatenate([down_own, down_other], axis=1),
        jnp.concatenate([down_other, down_own], axis=1),
    )
    down_sum = down_one + dot_rows(hidden[F1:], rows_two)
    down_norms = jnp.sum(down_sum * down_sum, axis=1)

    back_sum = combine_one(by_token, back_one)
    token_grad, gates_grad = combine_two(by_token, experts, gate, back_sum, back_two)
    return (
        token_grad,
        gates_grad,
        gate_grad[None],
        up_grad[None],
        down_sum.astype(BF)[None],
        norms[0:1],
        norms[1:2],
        down_norms[None],
    )


def solution(mesh):
    placed = (
        P("ep", "tp"),
        P("ep", "tp"),
        P("ep", None),
        P("ep", None),
        P("ep", None, "tp"),
        P("ep", None, "tp"),
        P("ep", "tp", None),
    )
    return jax.shard_map(
        step,
        mesh=mesh,
        in_specs=placed,
        out_specs=(
            P("ep", "tp"),
            P("ep", None),
            P("ep", None, "tp"),
            P("ep", None, "tp"),
            P("ep", "tp", None),
            P("ep", None),
            P("ep", None),
            P("ep", "tp"),
        ),
        check_vma=False,
    )
```

profile of v0, /device:TPU:0, one launch (start us, length us, event | category | flops | bytes accessed | tf_op | source)
XLA Modules:
  0.0 258.1 jit_solution(7714559750607762756)
XLA Ops:
  0.6 0.0 copy-start
  0.6 7.2 %send_tokens.1 = (bf16[64,8,3456]{2,1,0:T(8,128)(2,1)}, f32[512,384]{1,0:T(8,128)}, f32[512,384]{1,0:T(8,128)}) custom-call(s32[2,384]{1,0:T(2,128)} %bitcast.76, f32[2,384]{1,0:T(2,128)} %bitcast.77, bf16[384,1536]{1,0:T(8,128)(2,1)} %src_ref.3), custom_call_target="tpu_custom_call" | custom-call | tf_op jit(solution)/shard_map/send_tokens/pallas_call | solution.py:120
  7.9 11.8 %all-to-all-start.1 = ((bf16[64,8,3456]{2,1,0:T(8,128)(2,1)}), bf16[64,8,3456]{2,1,0:T(8,128)(2,1)}, u32[]{:S(2)}, u32[]{:S(2)}) async-start(bf16[64,8,3456]{2,1,0:T(8,128)(2,1)} %get-tuple-element.18), calls=%async_computation.1 | async-start | bytes 7077888 | tf_op jit(solution)/shard_map/all_to_all | solution.py:373
  19.7 6.0 %send.3 = bf16[64,8,1920]{2,1,0:T(8,128)(2,1)} custom-call(f32[512,384]{1,0:T(8,128)} %get-tuple-element.16.ranks_ref, f32[512,384]{1,0:T(8,128)} %get-tuple-element.17.gates_ref, bf16[384,1536]{1,0:T(8,128)(2,1)} %src_ref.5), custom_call_target="tpu_custom_call" | custom-call | tf_op jit(solution)/shard_map/send/pallas_call | solution.py:159
  25.7 39.8 %all-to-all-done.1.own_ref.own_last_ref = bf16[64,8,3456]{2,1,0:T(8,128)(2,1)} async-done(((bf16[64,8,3456]{2,1,0:T(8,128)(2,1)}), bf16[64,8,3456]{2,1,0:T(8,128)(2,1)}, u32[]{:S(2)}, u32[]{:S(2)}) %all-to-all-start.1) | async-done | bytes 3538976 | tf_op jit(solution)/shard_map/all_to_all | solution.py:373
  65.4 8.0 %all-to-all-start.3 = ((bf16[64,8,1920]{2,1,0:T(8,128)(2,1)}), bf16[64,8,1920]{2,1,0:T(8,128)(2,1)}, u32[]{:S(2)}, u32[]{:S(2)}) async-start(bf16[64,8,1920]{2,1,0:T(8,128)(2,1)} %send.3), calls=%async_computation.3 | async-start | bytes 3932160 | tf_op jit(solution)/shard_map/all_to_all | solution.py:373
  73.5 0.1 collective-permute-start.1
  73.6 28.5 %all-to-all-done.3.own_ref.own_last_ref = bf16[64,8,1920]{2,1,0:T(8,128)(2,1)} async-done(((bf16[64,8,1920]{2,1,0:T(8,128)(2,1)}), bf16[64,8,1920]{2,1,0:T(8,128)(2,1)}, u32[]{:S(2)}, u32[]{:S(2)}) %all-to-all-start.3) | async-done | bytes 1966112 | tf_op jit(solution)/shard_map/all_to_all | solution.py:373
  102.1 0.0 collective-permute-start.3
  102.1 4.5 %send.2 = bf16[64,8,1536]{2,1,0:T(8,128)(2,1)} custom-call(f32[512,384]{1,0:T(8,128)} %get-tuple-element.16.ranks_ref, f32[512,384]{1,0:T(8,128)} %get-tuple-element.17.gates_ref, bf16[384,1536]{1,0:T(8,128)(2,1)} %src_ref.5), custom_call_target="tpu_custom_call" | custom-call | tf_op jit(solution)/shard_map/send/pallas_call | solution.py:159
  106.6 5.9 %all-to-all-start = ((bf16[64,8,1536]{2,1,0:T(8,128)(2,1)}), bf16[64,8,1536]{2,1,0:T(8,128)(2,1)}, u32[]{:S(2)}, u32[]{:S(2)}) async-start(bf16[64,8,1536]{2,1,0:T(8,128)(2,1)} %send.2), calls=%async_computation | async-start | bytes 3145728 | tf_op jit(solution)/shard_map/all_to_all | solution.py:373
  112.6 25.0 %all-to-all-done = bf16[64,8,1536]{2,1,0:T(8,128)(2,1)} async-done(((bf16[64,8,1536]{2,1,0:T(8,128)(2,1)}), bf16[64,8,1536]{2,1,0:T(8,128)(2,1)}, u32[]{:S(2)}, u32[]{:S(2)}) %all-to-all-start) | async-done | bytes 1572896 | tf_op jit(solution)/shard_map/all_to_all | solution.py:373
  137.5 0.0 collective-permute-start
  137.5 3.6 %fusion.17 = f32[512,384]{1,0:T(8,128)} fusion(bf16[64,8,1536]{2,1,0:T(8,128)(2,1)} %all-to-all-done, bf16[1,384,3072]{2,1,0:T(8,128)(2,1)} %param.13, s32[]{:T(128)S(6)} %select_n.18), kind=kOutput, calls=%fused_computation.28 | convolution fusion | flops 603979776 | bytes 3538948 | tf_op jit(solution)/shard_map/dot_general | solution.py:29
  141.2 0.0 collective-permute-done.3.other_ref.other_last_ref
  141.2 5.7 %unpack.3 = bf16[640,3072]{1,0:T(8,128)(2,1)} custom-call(s32[1]{0:T(128)} %bitcast.6.core_ref, bf16[64,8,1920]{2,1,0:T(8,128)(2,1)} %all-to-all-done.3.own_ref.own_last_ref, bf16[64,8,1920]{2,1,0:T(8,128)(2,1)} %collective-permute-done.3.other_ref.other_last_ref, bf16[64,8,1920]{2,1,0:T(8,128)(2,1)} %all-to-all-done.3.own_ref.own_last_ref, ...), custom_call_target="tpu_custom_call" | custom-call | tf_op jit(solution)/shard_map/unpack/pallas_call | solution.py:207
  146.9 0.0 collective-permute-done.1.other_ref.other_last_ref
  146.9 9.4 %unpack.2.x_ref = bf16[1152,3072]{1,0:T(8,128)(2,1)} custom-call(s32[1]{0:T(128)} %bitcast.6.core_ref, bf16[64,8,3456]{2,1,0:T(8,128)(2,1)} %all-to-all-done.1.own_ref.own_last_ref, bf16[64,8,3456]{2,1,0:T(8,128)(2,1)} %collective-permute-done.1.other_ref.other_last_ref, bf16[64,8,3456]{2,1,0:T(8,128)(2,1)} %all-to-all-done.1.own_ref.own_last_ref, ...), custom_call_target="tpu_custom_call" | custom-call | tf_op jit(solution)/shard_map/unpack/pallas_call | solution.py:207
  156.3 6.9 %fusion.6 = f32[1152,384]{1,0:T(8,128)S(1)} fusion(bf16[1152,3072]{1,0:T(8,128)(2,1)} %unpack.2.x_ref, bf16[1,3072,384]{2,1,0:T(8,128)(2,1)} %param.11), kind=kOutput, calls=%fused_computation.13 | convolution fusion | flops 2717908992 | bytes 11206656 | tf_op jit(solution)/shard_map/dot_general | solution.py:25
  163.2 0.0 copy-start.12
  163.2 0.0 copy-start.13
  163.2 4.4 %multiply_convert_fusion = (bf16[1152,384]{1,0:T(8,128)(2,1)S(1)}, f32[1152,384]{1,0:T(8,128)S(1)}, f32[1152,384]{1,0:T(8,128)S(1)}) fusion(f32[1152,384]{1,0:T(8,128)S(1)} %fusion.6, bf16[1152,3072]{1,0:T(8,128)(2,1)S(1)} %copy-done.1, bf16[1,3072,384]{2,1,0:T(8,128)(2,1)S(1)} %copy-done), kind=kOutput, calls=%fused_computation.18 | convolution fusion | flops 2722775040 | bytes 15630336 | tf_op jit(solution)/shard_map/dot_general | solution.py:25
  167.7 0.0 copy-start.10
  167.7 0.0 collective-permute-done
  167.7 0.0 copy-start.3
  167.7 2.9 %multiply_reduce_fusion.2 = (f32[512]{0:T(512)S(1)}, bf16[512,384]{1,0:T(8,128)(2,1)S(1)}, bf16[512,384]{1,0:T(8,128)(2,1)S(1)}) fusion(bf16[1152,384]{1,0:T(8,128)(2,1)S(1)} %get-tuple-element.34, f32[1152,384]{1,0:T(8,128)S(1)} %get-tuple-element.36, f32[1152,384]{1,0:T(8,128)S(1)} %get-tuple-element.35, f32[512,384]{1,0:T(8,128)S(1)} %copy-done.12, ...), kind=kOutput, calls=%fused_computation.64 | convolution fusion | flops 605552128 | bytes 6293508 | tf_op jit(solution)/shard_map/dot_general | solution.py:29
  170.6 1.0 fusion.26
  171.6 1.0 fusion.2
  172.7 0.8 collective-permute-start.2
  173.5 0.3 copy-done.8
  173.8 2.3 multiply_reduce_fusion.1
  176.1 1.2 fusion.24
  177.3 2.5 add_convert_fusion
  179.8 0.5 collective-permute-start.4
  180.3 1.0 fusion.32
  181.3 0.0 collective-permute-done.2
  181.3 2.2 fusion.3
  183.6 5.5 %all-to-all-start.2 = ((bf16[64,8,1536]{2,1,0:T(8,128)(2,1)}), bf16[64,8,1536]{2,1,0:T(8,128)(2,1)}, u32[]{:S(2)}, u32[]{:S(2)}) async-start(bf16[64,8,1536]{2,1,0:T(8,128)(2,1)} %fusion.3), calls=%async_computation.2 | async-start | bytes 3145728 | tf_op jit(solution)/shard_map/all_to_all | solution.py:373
  189.2 0.0 copy-start.15
  189.2 0.1 collective-permute-start.5
  189.3 2.5 fusion.30
  191.8 2.5 add_convert_fusion.1.mine_ref.mine_last_ref
  194.4 0.0 collective-permute-done.5.got_part_ref
  194.4 0.0 collective-permute-done.4.got_ref.got_last_ref
  194.4 0.6 copy-done.18
  194.9 5.1 %pack.1 = bf16[64,8,2048]{2,1,0:T(8,128)(2,1)} custom-call(bf16[640,1536]{1,0:T(8,128)(2,1)} %add_convert_fusion.1.mine_ref.mine_last_ref, bf16[640,1536]{1,0:T(8,128)(2,1)} %collective-permute-done.4.got_ref.got_last_ref, bf16[640,1536]{1,0:T(8,128)(2,1)} %add_convert_fusion.1.mine_ref.mine_last_ref, ...), custom_call_target="tpu_custom_call" | custom-call | tf_op jit(solution)/shard_map/pack/pallas_call | solution.py:244
  200.0 13.9 %all-to-all-done.2.one_ref = bf16[64,8,1536]{2,1,0:T(8,128)(2,1)} async-done(((bf16[64,8,1536]{2,1,0:T(8,128)(2,1)}), bf16[64,8,1536]{2,1,0:T(8,128)(2,1)}, u32[]{:S(2)}, u32[]{:S(2)}) %all-to-all-start.2) | async-done | bytes 1572896 | tf_op jit(solution)/shard_map/all_to_all | solution.py:373
  213.9 5.6 %all-to-all-start.4 = ((bf16[64,8,2048]{2,1,0:T(8,128)(2,1)}), bf16[64,8,2048]{2,1,0:T(8,128)(2,1)}, u32[]{:S(2)}, u32[]{:S(2)}) async-start(bf16[64,8,2048]{2,1,0:T(8,128)(2,1)} %pack.1), calls=%async_computation.4 | async-start | bytes 4194304 | tf_op jit(solution)/shard_map/all_to_all | solution.py:373
  219.5 0.8 copy.15.exp_ref
  220.3 0.8 copy.27.gate_ref
  221.1 2.4 token_ranks.1.ranks_ref
  223.5 11.3 %weight_grads.1 = (bf16[3072,384]{1,0:T(8,128)(2,1)}, bf16[3072,384]{1,0:T(8,128)(2,1)}, f32[2,3072]{1,0:T(2,128)}) custom-call(bf16[1152,3072]{1,0:T(8,128)(2,1)} %unpack.2.x_ref, bf16[512,384]{1,0:T(8,128)(2,1)} %copy-done.2, bf16[512,384]{1,0:T(8,128)(2,1)} %copy-done.5, bf16[640,384]{1,0:T(8,128)(2,1)} %copy-done.4, bf16[640,384]{1,0:T(8,128)(2,1)} %copy-done.6), custom_call_target="tpu_custom_call" | custom-call | tf_op jit(solution)/shard_map/weight_grads/pallas_call | solution.py:361
  234.8 0.0 collective-permute-start.6
  234.8 2.2 fusion.11
  237.0 2.4 fusion.15
  239.4 0.2 copy-done.9
  239.6 4.5 %multiply_reduce_fusion = (f32[384]{0:T(512)S(1)}, bf16[1,384,3072]{2,1,0:T(8,128)(2,1)}) fusion(bf16[640,3072]{1,0:T(8,128)(2,1)S(1)} %copy-done.9, bf16[1152,384]{1,0:T(8,128)(2,1)S(1)} %copy-done.11, f32[384,1536]{1,0:T(8,128)S(1)} %fusion.15, f32[384,1536]{1,0:T(8,128)S(1)} %fusion.11, pred[]{:T(512)S(6)} %eq.3), kind=kOutput, calls=%fused_computation.2 | convolution fusion | flops 1518206592 | bytes 11503105 | tf_op jit(solution)/shard_map/dot_general | solution.py:33
  244.1 0.6 broadcast_in_dim.15
  244.7 0.0 collective-permute-done.6
  244.7 0.6 fusion.63
  245.4 4.7 %combine_one.1.sum_ref = f32[384,1536]{1,0:T(8,128)} custom-call(f32[384,512]{1,0:T(8,128)} %token_ranks.1.ranks_ref, bf16[64,8,1536]{2,1,0:T(8,128)(2,1)} %all-to-all-done.2.one_ref), custom_call_target="tpu_custom_call" | custom-call | tf_op jit(solution)/shard_map/combine_one/pallas_call | solution.py:285
  250.1 0.0 all-to-all-done.4.two_ref.last_ref.prod_ref
  250.1 6.4 %combine_two.1 = (bf16[384,1536]{1,0:T(8,128)(2,1)}, f32[384,2]{1,0:T(8,128)}) custom-call(f32[384,512]{1,0:T(8,128)} %token_ranks.1.ranks_ref, s32[384,2]{1,0:T(8,128)} %copy.15.exp_ref, f32[384,2]{1,0:T(8,128)} %copy.27.gate_ref, f32[384,1536]{1,0:T(8,128)} %combine_one.1.sum_ref, bf16[64,8,2048]{2,1,0:T(8,128)(2,1)} %all-to-all-done.4.two_ref.last_ref.prod_ref, ...), custom_call_target="tpu_custom_call" | custom-call | tf_op jit(solution)/shard_map/combine_two/pallas_call | solution.py:323
  256.5 1.6 copy.28
  (32 shorter events, 0.1 us)
Async XLA Ops:
  0.6 162.5 %copy-start = (bf16[1,3072,384]{2,1,0:T(8,128)(2,1)S(1)}, bf16[1,3072,384]{2,1,0:T(8,128)(2,1)}, u32[]{:S(2)}) copy-start(bf16[1,3072,384]{2,1,0:T(8,128)(2,1)} %param.12) | copy-start | bytes 7077892
  7.9 57.5 %all-to-all-start.1 = ((bf16[64,8,3456]{2,1,0:T(8,128)(2,1)}), bf16[64,8,3456]{2,1,0:T(8,128)(2,1)}, u32[]{:S(2)}, u32[]{:S(2)}) async-start(bf16[64,8,3456]{2,1,0:T(8,128)(2,1)} %get-tuple-element.18), calls=%async_computation.1 | async-start | bytes 7077888 | tf_op jit(solution)/shard_map/all_to_all | solution.py:373
  65.4 36.7 %all-to-all-start.3 = ((bf16[64,8,1920]{2,1,0:T(8,128)(2,1)}), bf16[64,8,1920]{2,1,0:T(8,128)(2,1)}, u32[]{:S(2)}, u32[]{:S(2)}) async-start(bf16[64,8,1920]{2,1,0:T(8,128)(2,1)} %send.3), calls=%async_computation.3 | async-start | bytes 3932160 | tf_op jit(solution)/shard_map/all_to_all | solution.py:373
  73.5 73.4 %collective-permute-start.1 = (bf16[64,8,3456]{2,1,0:T(8,128)(2,1)}, bf16[64,8,3456]{2,1,0:T(8,128)(2,1)}, u32[]{:S(2)}, u32[]{:S(2)}) collective-permute-start(bf16[64,8,3456]{2,1,0:T(8,128)(2,1)} %all-to-all-done.1.own_ref.own_last_ref), channel_id=1, source_target_pairs={{0,1},{1,0},{2,3},{3,2},{4,5},{5,4},{6,7},{7,6},{8,9},{9,8},{10,11... | collective-permute-start | bytes 10616840 | tf_op jit(solution)/shard_map/ppermute | solution.py:377
  102.1 39.1 %collective-permute-start.3 = (bf16[64,8,1920]{2,1,0:T(8,128)(2,1)}, bf16[64,8,1920]{2,1,0:T(8,128)(2,1)}, u32[]{:S(2)}, u32[]{:S(2)}) collective-permute-start(bf16[64,8,1920]{2,1,0:T(8,128)(2,1)} %all-to-all-done.3.own_ref.own_last_ref), channel_id=1, source_target_pairs={{0,1},{1,0},{2,3},{3,2},{4,5},{5,4},{6,7},{7,6},{8,9},{9,8},{10,11... | collective-permute-start | bytes 5898248 | tf_op jit(solution)/shard_map/ppermute | solution.py:377
  106.6 30.9 %all-to-all-start = ((bf16[64,8,1536]{2,1,0:T(8,128)(2,1)}), bf16[64,8,1536]{2,1,0:T(8,128)(2,1)}, u32[]{:S(2)}, u32[]{:S(2)}) async-start(bf16[64,8,1536]{2,1,0:T(8,128)(2,1)} %send.2), calls=%async_computation | async-start | bytes 3145728 | tf_op jit(solution)/shard_map/all_to_all | solution.py:373
  137.5 30.1 %collective-permute-start = (bf16[64,8,1536]{2,1,0:T(8,128)(2,1)}, bf16[64,8,1536]{2,1,0:T(8,128)(2,1)}, u32[]{:S(2)}, u32[]{:S(2)}) collective-permute-start(bf16[64,8,1536]{2,1,0:T(8,128)(2,1)} %all-to-all-done), channel_id=1, source_target_pairs={{0,1},{1,0},{2,3},{3,2},{4,5},{5,4},{6,7},{7,6},{8,9},{9,8},{10,11... | collective-permute-start | bytes 4718600 | tf_op jit(solution)/shard_map/ppermute | solution.py:377
  156.3 6.9 %copy-start.1 = (bf16[1152,3072]{1,0:T(8,128)(2,1)S(1)}, bf16[1152,3072]{1,0:T(8,128)(2,1)}, u32[]{:S(2)}) copy-start(bf16[1152,3072]{1,0:T(8,128)(2,1)} %unpack.2.x_ref) | copy-start | bytes 21233668
  163.2 4.5 %copy-start.12 = (f32[512,384]{1,0:T(8,128)S(1)}, f32[512,384]{1,0:T(8,128)}, u32[]{:S(2)}) copy-start(f32[512,384]{1,0:T(8,128)} %fusion.17) | copy-start | bytes 2359300
  163.2 4.5 %copy-start.13 = (bf16[1,384,3072]{2,1,0:T(8,128)(2,1)S(1)}, bf16[1,384,3072]{2,1,0:T(8,128)(2,1)}, u32[]{:S(2)}) copy-start(bf16[1,384,3072]{2,1,0:T(8,128)(2,1)} %param.13) | copy-start | bytes 7077892
  167.7 5.8 %copy-start.10 = (bf16[1152,384]{1,0:T(8,128)(2,1)}, bf16[1152,384]{1,0:T(8,128)(2,1)S(1)}, u32[]{:S(2)}) copy-start(bf16[1152,384]{1,0:T(8,128)(2,1)S(1)} %get-tuple-element.34) | copy-start | bytes 2654212
  167.7 2.9 %copy-start.3 = (bf16[1,3072,384]{2,1,0:T(8,128)(2,1)S(1)}, bf16[1,3072,384]{2,1,0:T(8,128)(2,1)}, u32[]{:S(2)}) copy-start(bf16[1,3072,384]{2,1,0:T(8,128)(2,1)} %param.11) | copy-start | bytes 7077892
  170.6 9.7 %copy-start.2 = (bf16[512,384]{1,0:T(8,128)(2,1)}, bf16[512,384]{1,0:T(8,128)(2,1)S(1)}, u32[]{:S(2)}) copy-start(bf16[512,384]{1,0:T(8,128)(2,1)S(1)} %get-tuple-element.42.g1_ref) | copy-start | bytes 1179652
  170.6 10.7 %copy-start.5 = (bf16[512,384]{1,0:T(8,128)(2,1)}, bf16[512,384]{1,0:T(8,128)(2,1)S(1)}, u32[]{:S(2)}) copy-start(bf16[512,384]{1,0:T(8,128)(2,1)S(1)} %get-tuple-element.41.u1_ref) | copy-start | bytes 1179652
  171.6 2.1 copy-start.8
  172.7 8.6 %collective-permute-start.2 = (bf16[512,1536]{1,0:T(8,128)(2,1)S(1)}, bf16[512,1536]{1,0:T(8,128)(2,1)S(1)}, u32[]{:S(2)}, u32[]{:S(2)}) collective-permute-start(bf16[512,1536]{1,0:T(8,128)(2,1)S(1)} %fusion.2), channel_id=1, source_target_pairs={{0,1},{1,0},{2,3},{3,2},{4,5},{5,4},{6,7},{7,6},{8,9},{9,8},{10,11... | collective-permute-start | bytes 4718600 | tf_op jit(solution)/shard_map/ppermute | solution.py:377
  176.1 1.2 copy-start.6
  176.1 13.2 %copy-start.4 = (bf16[640,384]{1,0:T(8,128)(2,1)}, bf16[640,384]{1,0:T(8,128)(2,1)S(1)}, u32[]{:S(2)}) copy-start(bf16[640,384]{1,0:T(8,128)(2,1)S(1)} %get-tuple-element.39.g2_ref) | copy-start | bytes 1474564
  179.8 14.5 %collective-permute-start.4 = (bf16[640,1536]{1,0:T(8,128)(2,1)}, bf16[640,1536]{1,0:T(8,128)(2,1)}, u32[]{:S(2)}, u32[]{:S(2)}) collective-permute-start(bf16[640,1536]{1,0:T(8,128)(2,1)} %add_convert_fusion), channel_id=1, source_target_pairs={{0,1},{1,0},{2,3},{3,2},{4,5},{5,4},{6,7},{7,6},{8,9},{9,8},{10,11... | collective-permute-start | bytes 5898248 | tf_op jit(solution)/shard_map/ppermute | solution.py:377
  183.6 30.3 %all-to-all-start.2 = ((bf16[64,8,1536]{2,1,0:T(8,128)(2,1)}), bf16[64,8,1536]{2,1,0:T(8,128)(2,1)}, u32[]{:S(2)}, u32[]{:S(2)}) async-start(bf16[64,8,1536]{2,1,0:T(8,128)(2,1)} %fusion.3), calls=%async_computation.2 | async-start | bytes 3145728 | tf_op jit(solution)/shard_map/all_to_all | solution.py:373
  189.2 2.6 %copy-start.15 = (f32[1,1152]{1,0:T(1,128)}, f32[1,1152]{1,0:T(1,128)S(1)}, u32[]{:S(2)}) copy-start(f32[1,1152]{1,0:T(1,128)S(1)} %reshape.41.part_ref) | copy-start | bytes 13828
  189.2 2.6 %copy-start.7 = (bf16[640,384]{1,0:T(8,128)(2,1)S(1)}, bf16[640,384]{1,0:T(8,128)(2,1)}, u32[]{:S(2)}) copy-start(bf16[640,384]{1,0:T(8,128)(2,1)} %copy-done.6) | copy-start | bytes 1474564
  189.2 5.2 %collective-permute-start.5 = (f32[1,1152]{1,0:T(1,128)S(1)}, f32[1,1152]{1,0:T(1,128)S(1)}, u32[]{:S(2)}, u32[]{:S(2)}) collective-permute-start(f32[1,1152]{1,0:T(1,128)S(1)} %reshape.41.part_ref), channel_id=1, source_target_pairs={{0,1},{1,0},{2,3},{3,2},{4,5},{5,4},{6,7},{7,6},{8,9},{9,8},{10,11... | collective-permute-start | bytes 13832 | tf_op jit(solution)/shard_map/ppermute | solution.py:377
  194.4 0.6 copy-start.18
  200.0 19.4 %copy-start.16 = (s32[384,2]{0,1:T(2,128)S(1)}, s32[384,2]{0,1:T(2,128)}, u32[]{:S(2)}) copy-start(s32[384,2]{0,1:T(2,128)} %param.9) | copy-start | bytes 9220
  200.0 20.3 %copy-start.17 = (f32[384,2]{0,1:T(2,128)S(1)}, f32[384,2]{0,1:T(2,128)}, u32[]{:S(2)}) copy-start(f32[384,2]{0,1:T(2,128)} %param.10) | copy-start | bytes 9220
  213.9 36.2 %all-to-all-start.4 = ((bf16[64,8,2048]{2,1,0:T(8,128)(2,1)}), bf16[64,8,2048]{2,1,0:T(8,128)(2,1)}, u32[]{:S(2)}, u32[]{:S(2)}) async-start(bf16[64,8,2048]{2,1,0:T(8,128)(2,1)} %pack.1), calls=%async_computation.4 | async-start | bytes 4194304 | tf_op jit(solution)/shard_map/all_to_all | solution.py:373
  223.5 11.3 %copy-start.11 = (bf16[1152,384]{1,0:T(8,128)(2,1)S(1)}, bf16[1152,384]{1,0:T(8,128)(2,1)}, u32[]{:S(2)}) copy-start(bf16[1152,384]{1,0:T(8,128)(2,1)} %copy-done.10) | copy-start | bytes 2654212
  234.8 9.9 %collective-permute-start.6 = (f32[2,3072]{1,0:T(2,128)}, f32[2,3072]{1,0:T(2,128)S(1)}, u32[]{:S(2)}, u32[]{:S(2)}) collective-permute-start(f32[2,3072]{1,0:T(2,128)} %get-tuple-element.23), channel_id=1, source_target_pairs={{0,1},{1,0},{2,3},{3,2},{4,5},{5,4},{6,7},{7,6},{8,9},{9,8},{10,11... | collective-permute-start | bytes 73736 | tf_op jit(solution)/shard_map/ppermute | solution.py:377
  237.0 2.6 %copy-start.9 = (bf16[640,3072]{1,0:T(8,128)(2,1)S(1)}, bf16[640,3072]{1,0:T(8,128)(2,1)}, u32[]{:S(2)}) copy-start(bf16[640,3072]{1,0:T(8,128)(2,1)} %unpack.3) | copy-start | bytes 11796484
  239.6 5.1 %copy-start.14 = (f32[2,3072]{1,0:T(2,128)S(1)}, f32[2,3072]{1,0:T(2,128)}, u32[]{:S(2)}) copy-start(f32[2,3072]{1,0:T(2,128)} %get-tuple-element.23) | copy-start | bytes 73732
where the time goes:
time: 261 us; the launch traced here: 258 us
  waiting for transfers between devices  107 us (41%)
  Pallas kernels  62.8 us (24%)
  matrix products  43.2 us (17%)
  starting transfers between devices  38.3 us (15%)
  local copies, waits for them, and re-layouts  5.61 us (2%)
    all_to_all x5, waiting for transfers between devices, to_experts(): return lax.all_to_all(x, 'ep', split_axis=0, concat_axis=0, tiled=True)  107 us
    all_to_all x5, starting transfers between devices, to_experts(): return lax.all_to_all(x, 'ep', split_axis=0, concat_axis=0, tiled=True)  36.8 us
    dot_general x11, matrix products, dot_last(): lax.dot_general(a, b, (((1,), (1,)), ((), ())), preferred_element_type=F32)  22.9 us
    pallas_call x2, Pallas kernels, unpack(): pl.pallas_call(functools.partial(unpack_kernel, steps), grid=(steps + 1,)...  15.1 us
    dot_general x2, matrix products, dot(): lax.dot_general(a, b, (((1,), (0,)), ((), ())), preferred_element_type=F32)  11.3 us
    pallas_call x1, Pallas kernels, weight_grads(): pl.pallas_call(weight_grads_kernel, grid=(6,), in_specs=[pl.BlockSpec((11...  11.3 us
    pallas_call x2, Pallas kernels, send(): pl.pallas_call(functools.partial(send_kernel, lo, hi == 9), grid=(hi - lo...  10.5 us
    dot_general x3, matrix products, dot_rows(): lax.dot_general(a, b, (((0,), (0,)), ((), ())), preferred_element_type=F32)  9.07 us
  transfers between devices with their start and end apart: 12, of which 4 were waited for; matrix products, arithmetic and copies ran while one was open for 16% of the time, Pallas kernels for 15%

commit v1 on v0

--- a/solution.py
+++ b/solution.py
@@ -69,7 +69,7 @@
     return total
 
 
-def send_tokens_kernel(exp_ref, gate_ref, src_ref, out_ref, ranks_ref, gates_ref, small_ref):
+def send_tokens_kernel(exp_ref, gate_ref, src_ref, out_ref, ranks_ref, gates_ref, line_ref, small_ref):
     b = pl.program_id(0)
 
     @pl.when(b == 0)
@@ -79,6 +79,8 @@
         small = jnp.where(named > 0.5, ranks, -1.0).astype(BF)
         small_ref[...] = small
         ranks_ref[...] = spread_rows(small)
+        for k, mask in enumerate(named_by(exp)):
+            line_ref[k : k + 1, :] = jnp.sum(jnp.where(mask, ranks, 0.0), axis=0, keepdims=True)
 
     def rows(piece, lo, hi):
         hit = ones_where(ranks_ref[...] == row_slots(jnp.int32(piece))).astype(BF)
@@ -121,8 +123,13 @@
         send_tokens_kernel,
         grid=(3,),
         in_specs=[small, small, pl.BlockSpec((TOK, H), lambda b: (0, 0))],
-        out_specs=[pl.BlockSpec((E, 8, 1152), lambda b: (0, 0, b)), table, table],
-        out_shape=[jax.ShapeDtypeStruct((E, 8, 3456), BF), shape, shape],
+        out_specs=[pl.BlockSpec((E, 8, 1152), lambda b: (0, 0, b)), table, table, small],
+        out_shape=[
+            jax.ShapeDtypeStruct((E, 8, 3456), BF),
+            shape,
+            shape,
+            jax.ShapeDtypeStruct((2, TOK), F32),
+        ],
         scratch_shapes=[pltpu.VMEM((E, TOK), BF)],
         name="send_tokens",
     )(exp_t, gate_t, tokens)
@@ -176,26 +183,25 @@
     return pieces
 
 
-def unpack_kernel(steps, core_ref, own_ref, other_ref, own_last_ref, other_last_ref, out_ref):
+def fill_rows(steps, core_ref, own_ref, other_ref, own_last_ref, other_last_ref, rows_ref):
     b = pl.program_id(0)
     core = core_ref[0]
     sides = ((core, own_ref, own_last_ref), (1 - core, other_ref, other_last_ref))
 
     @pl.when(b < steps)
     def _():
-        for half, rows_ref, _ in sides:
-            rows = rows_ref[...].astype(F32).reshape(128, H).astype(BF)
-            out_ref[:, pl.ds(pl.multiple_of(half * H, H), H)] = rows
+        for half, part_ref, _ in sides:
+            rows = part_ref[...].astype(F32).reshape(128, H).astype(BF)
+            rows_ref[:, pl.ds(pl.multiple_of(half * H, H), H)] = rows
 
     @pl.when(b == steps)
     def _():
         for half, _, last_ref in sides:
             for q, piece in enumerate(unpack_last(last_ref[...])):
-                out_ref[:, pl.ds(pl.multiple_of(half * H + q * Q, Q), Q)] = piece
-
-
-def unpack(core, own, other):
-    wide = (own.shape[2] - Q) // H
+                rows_ref[:, pl.ds(pl.multiple_of(half * H + q * Q, Q), Q)] = piece
+
+
+def packed_specs(wide):
     steps = 4 * wide
 
     def rows_at(b):
@@ -204,14 +210,72 @@
 
     rows = pl.BlockSpec((16, 8, H), rows_at)
     last = pl.BlockSpec((E, 8, Q), lambda b: (0, 0, wide * 4))
-    return pl.pallas_call(
-        functools.partial(unpack_kernel, steps),
-        grid=(steps + 1,),
-        in_specs=[pl.BlockSpec(memory_space=pltpu.SMEM), rows, rows, last, last],
-        out_specs=pl.BlockSpec((128, 2 * H), lambda b: (b, 0)),
-        out_shape=jax.ShapeDtypeStruct((steps * 128 + 128, 2 * H), BF),
-        name="unpack",
-    )(core, own, other, own, other)
+    return [pl.BlockSpec(memory_space=pltpu.SMEM), rows, rows, last, last]
+
+
+def forward_kernel(core_ref, own_ref, other_ref, own_last_ref, other_last_ref, *refs):
+    gate_ref, up_ref, rows_ref, hidden_ref, active_ref, slope_ref = refs
+    fill_rows(8, core_ref, own_ref, other_ref, own_last_ref, other_last_ref, rows_ref)
+    rows = rows_ref[...]
+    gate_pre = dot(rows, gate_ref[...])
+    up_pre = dot(rows, up_ref[...])
+    sigma = jax.nn.sigmoid(gate_pre)
+    active = gate_pre * sigma
+    active_ref[...] = active
+    hidden_ref[...] = (active * up_pre).astype(BF)
+    slope_ref[...] = up_pre * sigma * (1.0 + gate_pre * (1.0 - sigma))
+
+
+def forward(core, own, other, gate_mat, up_mat):
+    weights = pl.BlockSpec((2 * H, Q), lambda b: (0, 0))
+    block = pl.BlockSpec((128, Q), lambda b: (b, 0))
+    return pl.pallas_call(
+        forward_kernel,
+        grid=(9,),
+        in_specs=packed_specs(2) + [weights, weights],
+        out_specs=[pl.BlockSpec((128, 2 * H), lambda b: (b, 0)), block, block, block],
+        out_shape=[
+            jax.ShapeDtypeStruct((1152, 2 * H), BF),
+            jax.ShapeDtypeStruct((1152, Q), BF),
+            jax.ShapeDtypeStruct((1152, Q), F32),
+            jax.ShapeDtypeStruct((1152, Q), F32),
+        ],
+        name="forward",
+    )(core, own, other, own, other, gate_mat, up_mat)
+
+
+def middle_kernel(core_ref, own_ref, other_ref, own_last_ref, other_last_ref, *refs):
+    down_ref, hidden_ref, active_ref, slope_ref, rows_ref, gate_ref, up_ref, part_ref = refs
+    fill_rows(4, core_ref, own_ref, other_ref, own_last_ref, other_last_ref, rows_ref)
+    grad = dot(rows_ref[...], down_ref[...])
+    part = jnp.sum(hidden_ref[...].astype(F32) * grad, axis=1, keepdims=True)
+    part_ref[...] = jnp.broadcast_to(part, (128, 128)).T[0:1, :]
+    gate_ref[...] = (grad * slope_ref[...]).astype(BF)
+    up_ref[...] = (grad * active_ref[...]).astype(BF)
+
+
+def middle(core, own, other, down_turned, hidden, active, slope):
+    late = pl.BlockSpec((128, Q), lambda b: (b + 4, 0))
+    block = pl.BlockSpec((128, Q), lambda b: (b, 0))
+    shape = jax.ShapeDtypeStruct((640, Q), BF)
+    return pl.pallas_call(
+        middle_kernel,
+        grid=(5,),
+        in_specs=packed_specs(1) + [pl.BlockSpec((2 * H, Q), lambda b: (0, 0)), late, late, late],
+        out_specs=[
+            pl.BlockSpec((128, 2 * H), lambda b: (b, 0)),
+            block,
+            block,
+            pl.BlockSpec((1, 128), lambda b: (0, b)),
+        ],
+        out_shape=[
+            jax.ShapeDtypeStruct((640, 2 * H), BF),
+            shape,
+            shape,
+            jax.ShapeDtypeStruct((1, 640), F32),
+        ],
+        name="middle",
+    )(core, own, other, own, other, down_turned, hidden, active, slope)
 
 
 def pack_kernel(mine_ref, got_ref, mine_last_ref, got_last_ref, part_ref, got_part_ref, out_ref):
@@ -284,18 +348,19 @@
 def combine_one(ranks, one):
     return pl.pallas_call(
         combine_one_kernel,
-        grid=(4,),
+        grid=(2,),
         in_specs=[
             pl.BlockSpec((TOK, F1), lambda b: (0, 0)),
-            pl.BlockSpec((E, 8, Q), lambda b: (0, 0, b)),
+            pl.BlockSpec((E, 8, 2 * Q), lambda b: (0, 0, b)),
         ],
-        out_specs=pl.BlockSpec((TOK, Q), lambda b: (0, b)),
+        out_specs=pl.BlockSpec((TOK, 2 * Q), lambda b: (0, b)),
         out_shape=jax.ShapeDtypeStruct((TOK, H), F32),
         name="combine_one",
     )(ranks, one)
 
 
-def combine_two_kernel(ranks_ref, exp_ref, gate_ref, sum_ref, two_ref, last_ref, prod_ref, out_ref, gate_out_ref):
+def combine_two_kernel(ranks_ref, line_ref, exp_ref, gate_ref, *refs):
+    sum_ref, two_ref, last_ref, prod_ref, out_ref, gate_out_ref = refs
     b = pl.program_id(0)
 
     @pl.when(b == 0)
@@ -303,13 +368,11 @@
         pick = ones_where(iota((E, F1), 1) == 8 * iota((E, F1), 0)).astype(BF)
         table = dot(pick, flat_rows(prod_ref)).astype(BF)
         for k in range(2):
-            exp = exp_ref[:, k : k + 1]
-            at = iota((TOK, F1), 1) == 8 * exp
-            rank = jnp.sum(jnp.where(at, ranks_ref[...], 0.0), axis=1, keepdims=True)
-            found = dot(ones_where(iota((TOK, E), 1) == exp).astype(BF), table)
-            here = iota((TOK, 128), 1).astype(F32) == rank
-            found = jnp.sum(jnp.where(here, found, 0.0), axis=1, keepdims=True)
-            gate_out_ref[:, k : k + 1] = found / gate_ref[:, k : k + 1]
+            named = ones_where(iota((E, TOK), 0) == exp_ref[k : k + 1, :]).astype(BF)
+            found = dot_rows(table, named)
+            here = iota((128, TOK), 0).astype(F32) == line_ref[k : k + 1, :]
+            found = jnp.sum(jnp.where(here, found, 0.0), axis=0, keepdims=True)
+            gate_out_ref[k : k + 1, :] = found / gate_ref[k : k + 1, :]
 
     ranks = ranks_ref[...]
     block = iota((TOK, F1), 1) % 8 // 2
@@ -318,13 +381,14 @@
     out_ref[...] = (total + dot(ones_where(hit).astype(BF), flat_rows(last_ref))).astype(BF)
 
 
-def combine_two(ranks, experts, gate, total, two):
-    small = pl.BlockSpec((TOK, 2), lambda b: (0, 0))
+def combine_two(ranks, lines, exp_t, gate_t, total, two):
+    small = pl.BlockSpec((2, TOK), lambda b: (0, 0))
     return pl.pallas_call(
         combine_two_kernel,
         grid=(4,),
         in_specs=[
             pl.BlockSpec((TOK, F1), lambda b: (0, 0)),
+            small,
             small,
             small,
             pl.BlockSpec((TOK, Q), lambda b: (0, b)),
@@ -333,9 +397,24 @@
             pl.BlockSpec((E, 8, 128), lambda b: (0, 0, 15)),
         ],
         out_specs=[pl.BlockSpec((TOK, Q), lambda b: (0, b)), small],
-        out_shape=[jax.ShapeDtypeStruct((TOK, H), BF), jax.ShapeDtypeStruct((TOK, 2), F32)],
+        out_shape=[jax.ShapeDtypeStruct((TOK, H), BF), jax.ShapeDtypeStruct((2, TOK), F32)],
         name="combine_two",
-    )(ranks, experts, gate, total, two, two, two)
+    )(ranks, lines, exp_t, gate_t, total, two, two, two)
+
+
+def turn_kernel(src_ref, out_ref):
+    out_ref[...] = src_ref[...].T
+
+
+def turn(mat):
+    return pl.pallas_call(
+        turn_kernel,
+        grid=(6,),
+        in_specs=[pl.BlockSpec((Q, 512), lambda b: (0, b))],
+        out_specs=pl.BlockSpec((512, Q), lambda b: (b, 0)),
+        out_shape=jax.ShapeDtypeStruct((2 * H, Q), BF),
+        name="turn",
+    )(mat)
 
 
 def weight_grads_kernel(x_ref, g1_ref, u1_ref, g2_ref, u2_ref, gate_ref, up_ref, norm_ref, turned_ref):
@@ -389,7 +468,8 @@
     gates = [half(gate_mat, index, 0) for index in (core, 1 - core)]
     ups = [half(up_mat, index, 0) for index in (core, 1 - core)]
     downs = [half(down_mat, index, 1) for index in (core, 1 - core)]
-    tok_own, ranks, gates_of = send_tokens(exp_t, gate_t, tokens)
+    down_turned = turn(down_mat)
+    tok_own, ranks, gates_of, lines = send_tokens(exp_t, gate_t, tokens)
     tok_own = to_experts(tok_own)
     cot_one = send(ranks, gates_of, cotangent, 0, 4)
     cot_one = to_experts(cot_one)
@@ -398,46 +478,38 @@
     cot_two = to_experts(cot_two)
     tok_other = swap_cores(tok_own)
 
-    rows_in = unpack(core_arg, tok_own, tok_other)
-    gate_pre = dot(rows_in, gate_mat)
-    up_pre = dot(rows_in, up_mat)
-    sigma = jax.nn.sigmoid(gate_pre)
-    active = gate_pre * sigma
-    hidden = (active * up_pre).astype(BF)
-    gate_slope = up_pre * sigma * (1.0 + gate_pre * (1.0 - sigma))
-
-    def chunk(rows, lo, hi):
-        grad = rows[0]
-        for part in rows[1:]:
-            grad = grad + part
-        parts = jnp.sum(hidden[lo:hi].astype(F32) * grad, axis=1)
-        gate_grad_pre = (grad * gate_slope[lo:hi]).astype(BF)
-        up_grad_pre = (grad * active[lo:hi]).astype(BF)
-
+    rows_in, hidden, active, gate_slope = forward(core_arg, tok_own, tok_other, gate_mat, up_mat)
+
+    def send_back(gate_grad_pre, up_grad_pre):
         def partial(index):
             return (dot_last(gate_grad_pre, gates[index]) + dot_last(up_grad_pre, ups[index])).astype(BF)
 
         sent = swap_cores(partial(1))
-        return parts, gate_grad_pre, up_grad_pre, partial(0), sent
+        return partial(0), sent
 
     cot_one_other = swap_cores(cot_one)
     own = cot_one.reshape(F1, H)
     other = cot_one_other.reshape(F1, H)
-    one = chunk((dot_last(own, downs[0]), dot_last(other, downs[1])), 0, F1)
-    back_one = (one[3].astype(F32) + one[4].astype(F32)).astype(BF).reshape(E, 8, H)
+    grad = dot_last(own, downs[0]) + dot_last(other, downs[1])
+    parts_one = jnp.sum(hidden[:F1].astype(F32) * grad, axis=1)
+    gate_one = (grad * gate_slope[:F1]).astype(BF)
+    up_one = (grad * active[:F1]).astype(BF)
+    mine, sent = send_back(gate_one, up_one)
+    back_one = (mine.astype(F32) + sent.astype(F32)).astype(BF).reshape(E, 8, H)
     back_one = to_experts(back_one)
 
     cot_two_other = swap_cores(cot_two)
-    rows_two = unpack(core_arg, cot_two, cot_two_other)
-    two = chunk((dot_last(rows_two, down_mat),), F1, 1152)
-    parts = jnp.concatenate([one[0], two[0]])
-    parts = parts.reshape(1, 1152)
-    back_two = pack(two[3], two[4], parts, swap_cores(parts))
+    rows_two, gate_two, up_two, parts_two = middle(
+        core_arg, cot_two, cot_two_other, down_turned, hidden, active, gate_slope
+    )
+    mine, sent = send_back(gate_two, up_two)
+    parts = jnp.concatenate([parts_one.reshape(1, F1), parts_two], axis=1)
+    back_two = pack(mine, sent, parts, swap_cores(parts))
     back_two = to_experts(back_two)
 
     down_own = dot_rows(hidden[:F1], own)
     down_other = dot_rows(hidden[:F1], other)
-    gate_grad, up_grad, norms = weight_grads(rows_in, one[1], one[2], two[1], two[2])
+    gate_grad, up_grad, norms = weight_grads(rows_in, gate_one, up_one, gate_two, up_two)
     norms = norms + swap_cores(norms)
     down_one = jnp.where(
         core == 0,
@@ -448,10 +520,10 @@
     down_norms = jnp.sum(down_sum * down_sum, axis=1)
 
     back_sum = combine_one(by_token, back_one)
-    token_grad, gates_grad = combine_two(by_token, experts, gate, back_sum, back_two)
+    token_grad, gates_grad = combine_two(by_token, lines, exp_t, gate_t, back_sum, back_two)
     return (
         token_grad,
-        gates_grad,
+        gates_grad.T,
         gate_grad[None],
         up_grad[None],
         down_sum.astype(BF)[None],

time: 261 us -> 257 us (0.985)
  Pallas kernels: 62.8 us -> 74.9 us
  matrix products: 43.2 us -> 32.7 us
  waiting for transfers between devices: 107 us -> 104 us
    pallas_call x3 -> x4, Pallas kernels: 19.8 us -> 32.6 us  [the longest x1 14.9 us: forward(): pl.pallas_call(forward_kernel, grid=(9,), in_specs=packed_specs(2) + [wei...]
    dot_general x2 -> x0, matrix products: 11.3 us -> none  [dot(): lax.dot_general(a, b, (((1,), (0,)), ((), ())), preferred_element_type=F32)]
    all_to_all x5, waiting for transfers between devices: 107 us -> 104 us  [to_experts(): return lax.all_to_all(x, 'ep', split_axis=0, concat_axis=0, tiled=True)]
    dot_general x11 -> x10, matrix products: 22.9 us -> 23.6 us  [dot_last(): lax.dot_general(a, b, (((1,), (1,)), ((), ())), preferred_element_type=F32)]
  transfers between devices with their start and end apart: 12 -> 12, of which waited for: 4 -> 5; matrix products, arithmetic and copies ran while one was open for 16% -> 14% of each run, Pallas kernels for 15% -> 20%
where the time goes in v1:
time: 257 us; the launch traced here: 255 us
  waiting for transfers between devices  104 us (40%)
  Pallas kernels  74.9 us (29%)
  starting transfers between devices  37.6 us (15%)
  matrix products  32.7 us (13%)
  local copies, waits for them, and re-layouts  5.17 us (2%)
    all_to_all x5, waiting for transfers between devices, to_experts(): return lax.all_to_all(x, 'ep', split_axis=0, concat_axis=0, tiled=True)  104 us
    all_to_all x5, starting transfers between devices, to_experts(): return lax.all_to_all(x, 'ep', split_axis=0, concat_axis=0, tiled=True)  36.3 us
    dot_general x10, matrix products, dot_last(): lax.dot_general(a, b, (((1,), (1,)), ((), ())), preferred_element_type=F32)  23.6 us
    pallas_call x1, Pallas kernels, forward(): pl.pallas_call(forward_kernel, grid=(9,), in_specs=packed_specs(2) + [wei...  14.9 us
    pallas_call x1, Pallas kernels, weight_grads(): pl.pallas_call(weight_grads_kernel, grid=(6,), in_specs=[pl.BlockSpec((11...  11.3 us
    pallas_call x2, Pallas kernels, send(): pl.pallas_call(functools.partial(send_kernel, lo, hi == 9), grid=(hi - lo...  10.6 us
    dot_general x3, matrix products, dot_rows(): lax.dot_general(a, b, (((0,), (0,)), ((), ())), preferred_element_type=F32)  9.07 us
    pallas_call x1, Pallas kernels, middle(): pl.pallas_call(middle_kernel, grid=(5,), in_specs=packed_specs(1) + [pl.B...  8.98 us
  transfers between devices with their start and end apart: 12, of which 5 were waited for; matrix products, arithmetic and copies ran while one was open for 14% of the time, Pallas kernels for 20%

profile of v1, /device:TPU:0, one launch (start us, length us, event | category | flops | bytes accessed | tf_op | source)
XLA Modules:
  0.0 255.1 jit_solution(12725560348354475080)
XLA Ops:
  0.6 7.1 %send_tokens.1 = (bf16[64,8,3456]{2,1,0:T(8,128)(2,1)}, f32[512,384]{1,0:T(8,128)}, f32[512,384]{1,0:T(8,128)}, f32[2,384]{1,0:T(2,128)}) custom-call(s32[2,384]{1,0:T(2,128)} %bitcast.68, f32[2,384]{1,0:T(2,128)} %bitcast.70, bf16[384,1536]{1,0:T(8,128)(2,1)} %src_ref.3), custom_call_target="tpu_custom_call" | custom-call | tf_op jit(solution)/shard_map/send_tokens/pallas_call | solution.py:122
  7.7 11.5 %all-to-all-start.1 = ((bf16[64,8,3456]{2,1,0:T(8,128)(2,1)}), bf16[64,8,3456]{2,1,0:T(8,128)(2,1)S(1)}, u32[]{:S(2)}, u32[]{:S(2)}) async-start(bf16[64,8,3456]{2,1,0:T(8,128)(2,1)} %get-tuple-element.28), calls=%async_computation.1 | async-start | bytes 7077888 | tf_op jit(solution)/shard_map/all_to_all | solution.py:452
  19.3 4.6 %send.2 = bf16[64,8,1536]{2,1,0:T(8,128)(2,1)} custom-call(f32[512,384]{1,0:T(8,128)} %get-tuple-element.26.ranks_ref, f32[512,384]{1,0:T(8,128)} %get-tuple-element.27.gates_ref, bf16[384,1536]{1,0:T(8,128)(2,1)} %src_ref.5), custom_call_target="tpu_custom_call" | custom-call | tf_op jit(solution)/shard_map/send/pallas_call | solution.py:166
  23.8 41.3 %all-to-all-done.1.own_ref.own_last_ref = bf16[64,8,3456]{2,1,0:T(8,128)(2,1)S(1)} async-done(((bf16[64,8,3456]{2,1,0:T(8,128)(2,1)}), bf16[64,8,3456]{2,1,0:T(8,128)(2,1)S(1)}, u32[]{:S(2)}, u32[]{:S(2)}) %all-to-all-start.1) | async-done | bytes 3538976 | tf_op jit(solution)/shard_map/all_to_all | solution.py:452
  65.2 8.1 %all-to-all-start = ((bf16[64,8,1536]{2,1,0:T(8,128)(2,1)}), bf16[64,8,1536]{2,1,0:T(8,128)(2,1)}, u32[]{:S(2)}, u32[]{:S(2)}) async-start(bf16[64,8,1536]{2,1,0:T(8,128)(2,1)} %send.2), calls=%async_computation | async-start | bytes 3145728 | tf_op jit(solution)/shard_map/all_to_all | solution.py:452
  73.2 0.1 collective-permute-start.1
  73.3 6.0 %send.3 = bf16[64,8,1920]{2,1,0:T(8,128)(2,1)} custom-call(f32[512,384]{1,0:T(8,128)} %get-tuple-element.26.ranks_ref, f32[512,384]{1,0:T(8,128)} %get-tuple-element.27.gates_ref, bf16[384,1536]{1,0:T(8,128)(2,1)} %src_ref.5), custom_call_target="tpu_custom_call" | custom-call | tf_op jit(solution)/shard_map/send/pallas_call | solution.py:166
  79.3 0.0 copy-done.1
  79.3 18.4 %all-to-all-done = bf16[64,8,1536]{2,1,0:T(8,128)(2,1)} async-done(((bf16[64,8,1536]{2,1,0:T(8,128)(2,1)}), bf16[64,8,1536]{2,1,0:T(8,128)(2,1)}, u32[]{:S(2)}, u32[]{:S(2)}) %all-to-all-start) | async-done | bytes 1572896 | tf_op jit(solution)/shard_map/all_to_all | solution.py:452
  97.7 5.5 %all-to-all-start.3 = ((bf16[64,8,1920]{2,1,0:T(8,128)(2,1)}), bf16[64,8,1920]{2,1,0:T(8,128)(2,1)}, u32[]{:S(2)}, u32[]{:S(2)}) async-start(bf16[64,8,1920]{2,1,0:T(8,128)(2,1)} %send.3), calls=%async_computation.3 | async-start | bytes 3932160 | tf_op jit(solution)/shard_map/all_to_all | solution.py:452
  103.3 0.1 collective-permute-start
  103.4 27.8 %all-to-all-done.3.own_ref.own_last_ref = bf16[64,8,1920]{2,1,0:T(8,128)(2,1)} async-done(((bf16[64,8,1920]{2,1,0:T(8,128)(2,1)}), bf16[64,8,1920]{2,1,0:T(8,128)(2,1)}, u32[]{:S(2)}, u32[]{:S(2)}) %all-to-all-start.3) | async-done | bytes 1966112 | tf_op jit(solution)/shard_map/all_to_all | solution.py:452
  131.2 0.0 collective-permute-start.3
  131.2 3.6 %fusion.10 = f32[512,384]{1,0:T(8,128)} fusion(bf16[64,8,1536]{2,1,0:T(8,128)(2,1)} %all-to-all-done, bf16[1,384,3072]{2,1,0:T(8,128)(2,1)} %param.13, s32[]{:T(128)S(6)} %select_n.18), kind=kOutput, calls=%fused_computation.18 | convolution fusion | flops 603979776 | bytes 3538948 | tf_op jit(solution)/shard_map/dot_general | solution.py:29
  134.8 0.0 collective-permute-done.1.other_ref.other_last_ref
  134.8 14.9 %forward.1 = (bf16[1152,3072]{1,0:T(8,128)(2,1)}, bf16[1152,384]{1,0:T(8,128)(2,1)}, f32[1152,384]{1,0:T(8,128)}, f32[1152,384]{1,0:T(8,128)}) custom-call(s32[1]{0:T(128)} %bitcast.6.core_ref, bf16[64,8,3456]{2,1,0:T(8,128)(2,1)} %copy-done.1, bf16[64,8,3456]{2,1,0:T(8,128)(2,1)} %collective-permute-done.1.other_ref.other_last_ref, ...), custom_call_target="tpu_custom_call" | custom-call | tf_op jit(solution)/shard_map/forward/pallas_call | solution.py:232
  149.7 0.0 collective-permute-done
  149.7 0.0 copy-start.3
  149.8 3.5 %multiply_reduce_fusion.1 = (f32[512]{0:T(512)S(1)}, bf16[512,384]{1,0:T(8,128)(2,1)S(1)}, bf16[512,384]{1,0:T(8,128)(2,1)S(1)}) fusion(bf16[1152,384]{1,0:T(8,128)(2,1)} %get-tuple-element.31.refs_1_, f32[1152,384]{1,0:T(8,128)} %get-tuple-element.30.refs_2_, f32[1152,384]{1,0:T(8,128)} %get-tuple-element.29.refs_3_, f32[512,384]{1,0:T(8,128)} %fusion.10, ...), kind=kOutput, calls=%fused_computation.45 | convolution fusion | flops 605552128 | bytes 6293508 | tf_op jit(solution)/shard_map/dot_general | solution.py:29
  153.2 0.0 copy-start.8
  153.3 0.0 copy-done.3
  153.3 0.0 copy-start.2
  153.3 1.0 fusion.19
  154.3 0.9 copy-done.2
  155.2 2.2 fusion.2
  157.4 0.5 collective-permute-start.2
  157.9 5.3 %turn.1.refs_0_ = bf16[3072,384]{1,0:T(8,128)(2,1)} custom-call(bf16[384,3072]{1,0:T(8,128)(2,1)} %bitcast.67), custom_call_target="tpu_custom_call" | custom-call | tf_op jit(solution)/shard_map/turn/pallas_call | solution.py:410
  163.2 0.0 collective-permute-done.3.other_ref.other_last_ref
  163.2 9.0 %middle.1 = (bf16[640,3072]{1,0:T(8,128)(2,1)}, bf16[640,384]{1,0:T(8,128)(2,1)}, bf16[640,384]{1,0:T(8,128)(2,1)}, f32[1,640]{1,0:T(1,128)}) custom-call(s32[1]{0:T(128)} %bitcast.6.core_ref, bf16[64,8,1920]{2,1,0:T(8,128)(2,1)} %all-to-all-done.3.own_ref.own_last_ref, bf16[64,8,1920]{2,1,0:T(8,128)(2,1)} %collective-permute-done.3.other_ref.other_last_ref, ...), custom_call_target="tpu_custom_call" | custom-call | tf_op jit(solution)/shard_map/middle/pallas_call | solution.py:261
  172.2 2.4 fusion.15
  174.6 2.5 add_convert_fusion
  177.1 0.0 collective-permute-start.4
  177.1 0.0 copy-done.6
  177.1 1.0 fusion.25
  178.1 0.0 collective-permute-done.2
  178.1 0.0 copy-done.8
  178.2 3.6 %fusion.3 = bf16[64,8,1536]{2,1,0:T(8,128)(2,1)} fusion(bf16[512,1536]{1,0:T(8,128)(2,1)} %collective-permute-done.2, f32[512,1536]{1,0:T(8,128)S(1)} %fusion.25, bf16[512,384]{1,0:T(8,128)(2,1)S(1)} %get-tuple-element.45.u1_ref, bf16[1,3072,384]{2,1,0:T(8,128)(2,1)S(1)} %copy-done.2, s32[]{:T(128)S(6)} %select_n.18), kind=kOutput, calls=%fused_computation.10 | convolution fusion | flops 608698368 | bytes 7864324 | tf_op jit(solution)/shard_map/dot_general | solution.py:29
  181.8 5.9 %all-to-all-start.2 = ((bf16[64,8,1536]{2,1,0:T(8,128)(2,1)}), bf16[64,8,1536]{2,1,0:T(8,128)(2,1)}, u32[]{:S(2)}, u32[]{:S(2)}) async-start(bf16[64,8,1536]{2,1,0:T(8,128)(2,1)} %fusion.3), calls=%async_computation.2 | async-start | bytes 3145728 | tf_op jit(solution)/shard_map/all_to_all | solution.py:452
  187.8 0.0 copy-start.15
  187.8 0.0 copy-start.5
  187.8 0.5 collective-permute-start.5
  188.3 1.2 fusion.21
  189.6 2.5 add_convert_fusion.1.mine_ref.mine_last_ref
  192.1 0.0 collective-permute-done.5.got_part_ref
  192.1 0.0 collective-permute-done.4.got_ref.got_last_ref
  192.1 0.6 copy-done.16
  192.7 5.0 %pack.1 = bf16[64,8,2048]{2,1,0:T(8,128)(2,1)} custom-call(bf16[640,1536]{1,0:T(8,128)(2,1)} %add_convert_fusion.1.mine_ref.mine_last_ref, bf16[640,1536]{1,0:T(8,128)(2,1)} %collective-permute-done.4.got_ref.got_last_ref, bf16[640,1536]{1,0:T(8,128)(2,1)} %add_convert_fusion.1.mine_ref.mine_last_ref, ...), custom_call_target="tpu_custom_call" | custom-call | tf_op jit(solution)/shard_map/pack/pallas_call | solution.py:308
  197.7 15.0 %all-to-all-done.2.one_ref = bf16[64,8,1536]{2,1,0:T(8,128)(2,1)} async-done(((bf16[64,8,1536]{2,1,0:T(8,128)(2,1)}), bf16[64,8,1536]{2,1,0:T(8,128)(2,1)}, u32[]{:S(2)}, u32[]{:S(2)}) %all-to-all-start.2) | async-done | bytes 1572896 | tf_op jit(solution)/shard_map/all_to_all | solution.py:452
  212.7 5.3 %all-to-all-start.4 = ((bf16[64,8,2048]{2,1,0:T(8,128)(2,1)}), bf16[64,8,2048]{2,1,0:T(8,128)(2,1)S(1)}, u32[]{:S(2)}, u32[]{:S(2)}) async-start(bf16[64,8,2048]{2,1,0:T(8,128)(2,1)} %pack.1), calls=%async_computation.4 | async-start | bytes 4194304 | tf_op jit(solution)/shard_map/all_to_all | solution.py:452
  218.0 0.8 copy.15.exp_ref
  218.9 2.4 token_ranks.1.ranks_ref
  221.3 11.3 %weight_grads.1 = (bf16[3072,384]{1,0:T(8,128)(2,1)}, bf16[3072,384]{1,0:T(8,128)(2,1)}, f32[2,3072]{1,0:T(2,128)}) custom-call(bf16[1152,3072]{1,0:T(8,128)(2,1)} %get-tuple-element.37.x_ref, bf16[512,384]{1,0:T(8,128)(2,1)} %copy-done.6, bf16[512,384]{1,0:T(8,128)(2,1)} %copy-done.8, bf16[640,384]{1,0:T(8,128)(2,1)} %get-tuple-element.32.g2_ref, ...), custom_call_target="tpu_custom_call" | custom-call | tf_op jit(solution)/shard_map/weight_grads/pallas_call | solution.py:440
  232.6 0.0 collective-permute-start.6
  232.6 2.2 fusion.4
  234.8 2.4 fusion.8
  237.2 0.2 copy-done.18
  237.4 4.5 %multiply_reduce_fusion = (f32[384]{0:T(512)S(1)}, bf16[1,384,3072]{2,1,0:T(8,128)(2,1)}) fusion(bf16[640,3072]{1,0:T(8,128)(2,1)S(1)} %copy-done.18, bf16[1152,384]{1,0:T(8,128)(2,1)S(1)} %copy-done.9, f32[384,1536]{1,0:T(8,128)S(1)} %fusion.8, f32[384,1536]{1,0:T(8,128)S(1)} %fusion.4, pred[]{:T(512)S(6)} %eq.3), kind=kOutput, calls=%fused_computation.2 | convolution fusion | flops 1518206592 | bytes 11503105 | tf_op jit(solution)/shard_map/dot_general | solution.py:33
  241.9 0.6 broadcast_in_dim.15
  242.5 0.0 collective-permute-done.6
  242.5 0.6 fusion.52
  243.1 3.5 %combine_one.1.refs_0_ = f32[384,1536]{1,0:T(8,128)} custom-call(f32[384,512]{1,0:T(8,128)} %token_ranks.1.ranks_ref, bf16[64,8,1536]{2,1,0:T(8,128)(2,1)} %all-to-all-done.2.one_ref), custom_call_target="tpu_custom_call" | custom-call | tf_op jit(solution)/shard_map/combine_one/pallas_call | solution.py:349
  246.6 1.3 all-to-all-done.4.refs_1_.refs_2_.refs_3_
  247.9 1.4 copy-done
  249.2 5.9 %combine_two.1 = (bf16[384,1536]{1,0:T(8,128)(2,1)}, f32[2,384]{1,0:T(2,128)}) custom-call(f32[384,512]{1,0:T(8,128)} %token_ranks.1.ranks_ref, f32[2,384]{1,0:T(2,128)} %get-tuple-element.25.line_ref, s32[2,384]{1,0:T(2,128)} %bitcast.69, f32[2,384]{1,0:T(2,128)} %bitcast.71, f32[384,1536]{1,0:T(8,128)} %combine_one.1.refs_0_, ...), custom_call_target="tpu_custom_call" | custom-call | tf_op jit(solution)/shard_map/combine_two/pallas_call | solution.py:386
  (27 shorter events, 0.1 us)
Async XLA Ops:
  7.7 57.4 %all-to-all-start.1 = ((bf16[64,8,3456]{2,1,0:T(8,128)(2,1)}), bf16[64,8,3456]{2,1,0:T(8,128)(2,1)S(1)}, u32[]{:S(2)}, u32[]{:S(2)}) async-start(bf16[64,8,3456]{2,1,0:T(8,128)(2,1)} %get-tuple-element.28), calls=%async_computation.1 | async-start | bytes 7077888 | tf_op jit(solution)/shard_map/all_to_all | solution.py:452
  65.2 14.2 %copy-start.1 = (bf16[64,8,3456]{2,1,0:T(8,128)(2,1)}, bf16[64,8,3456]{2,1,0:T(8,128)(2,1)S(1)}, u32[]{:S(2)}) copy-start(bf16[64,8,3456]{2,1,0:T(8,128)(2,1)S(1)} %all-to-all-done.1.own_ref.own_last_ref) | copy-start | bytes 10616836
  65.2 32.5 %all-to-all-start = ((bf16[64,8,1536]{2,1,0:T(8,128)(2,1)}), bf16[64,8,1536]{2,1,0:T(8,128)(2,1)}, u32[]{:S(2)}, u32[]{:S(2)}) async-start(bf16[64,8,1536]{2,1,0:T(8,128)(2,1)} %send.2), calls=%async_computation | async-start | bytes 3145728 | tf_op jit(solution)/shard_map/all_to_all | solution.py:452
  73.2 61.6 %collective-permute-start.1 = (bf16[64,8,3456]{2,1,0:T(8,128)(2,1)S(1)}, bf16[64,8,3456]{2,1,0:T(8,128)(2,1)}, u32[]{:S(2)}, u32[]{:S(2)}) collective-permute-start(bf16[64,8,3456]{2,1,0:T(8,128)(2,1)S(1)} %all-to-all-done.1.own_ref.own_last_ref), channel_id=1, source_target_pairs={{0,1},{1,0},{2,3},{3,2},{4,5},{5,4},{6,7},{7,6},{8,9},{9,8},{10,11... | collective-permute-start | bytes 10616840 | tf_op jit(solution)/shard_map/ppermute | solution.py:456
  97.7 33.5 %all-to-all-start.3 = ((bf16[64,8,1920]{2,1,0:T(8,128)(2,1)}), bf16[64,8,1920]{2,1,0:T(8,128)(2,1)}, u32[]{:S(2)}, u32[]{:S(2)}) async-start(bf16[64,8,1920]{2,1,0:T(8,128)(2,1)} %send.3), calls=%async_computation.3 | async-start | bytes 3932160 | tf_op jit(solution)/shard_map/all_to_all | solution.py:452
  103.3 46.5 %collective-permute-start = (bf16[64,8,1536]{2,1,0:T(8,128)(2,1)}, bf16[64,8,1536]{2,1,0:T(8,128)(2,1)}, u32[]{:S(2)}, u32[]{:S(2)}) collective-permute-start(bf16[64,8,1536]{2,1,0:T(8,128)(2,1)} %all-to-all-done), channel_id=1, source_target_pairs={{0,1},{1,0},{2,3},{3,2},{4,5},{5,4},{6,7},{7,6},{8,9},{9,8},{10,11... | collective-permute-start | bytes 4718600 | tf_op jit(solution)/shard_map/ppermute | solution.py:456
  131.2 32.0 %collective-permute-start.3 = (bf16[64,8,1920]{2,1,0:T(8,128)(2,1)}, bf16[64,8,1920]{2,1,0:T(8,128)(2,1)}, u32[]{:S(2)}, u32[]{:S(2)}) collective-permute-start(bf16[64,8,1920]{2,1,0:T(8,128)(2,1)} %all-to-all-done.3.own_ref.own_last_ref), channel_id=1, source_target_pairs={{0,1},{1,0},{2,3},{3,2},{4,5},{5,4},{6,7},{7,6},{8,9},{9,8},{10,11... | collective-permute-start | bytes 5898248 | tf_op jit(solution)/shard_map/ppermute | solution.py:456
  134.8 14.9 %copy-start.10 = (bf16[1,384,3072]{2,1,0:T(8,128)(2,1)S(1)}, bf16[1,384,3072]{2,1,0:T(8,128)(2,1)}, u32[]{:S(2)}) copy-start(bf16[1,384,3072]{2,1,0:T(8,128)(2,1)} %param.13) | copy-start | bytes 7077892
  149.7 3.5 %copy-start.3 = (bf16[1,3072,384]{2,1,0:T(8,128)(2,1)S(1)}, bf16[1,3072,384]{2,1,0:T(8,128)(2,1)}, u32[]{:S(2)}) copy-start(bf16[1,3072,384]{2,1,0:T(8,128)(2,1)} %param.11) | copy-start | bytes 7077892
  153.2 23.9 %copy-start.6 = (bf16[512,384]{1,0:T(8,128)(2,1)}, bf16[512,384]{1,0:T(8,128)(2,1)S(1)}, u32[]{:S(2)}) copy-start(bf16[512,384]{1,0:T(8,128)(2,1)S(1)} %get-tuple-element.46.g1_ref) | copy-start | bytes 1179652
  153.2 24.9 %copy-start.8 = (bf16[512,384]{1,0:T(8,128)(2,1)}, bf16[512,384]{1,0:T(8,128)(2,1)S(1)}, u32[]{:S(2)}) copy-start(bf16[512,384]{1,0:T(8,128)(2,1)S(1)} %get-tuple-element.45.u1_ref) | copy-start | bytes 1179652
  153.3 1.9 copy-start.2
  157.4 20.7 %collective-permute-start.2 = (bf16[512,1536]{1,0:T(8,128)(2,1)}, bf16[512,1536]{1,0:T(8,128)(2,1)}, u32[]{:S(2)}, u32[]{:S(2)}) collective-permute-start(bf16[512,1536]{1,0:T(8,128)(2,1)} %fusion.2), channel_id=1, source_target_pairs={{0,1},{1,0},{2,3},{3,2},{4,5},{5,4},{6,7},{7,6},{8,9},{9,8},{10,11... | collective-permute-start | bytes 4718600 | tf_op jit(solution)/shard_map/ppermute | solution.py:456
  172.2 2.4 copy-start.4
  172.2 2.4 copy-start.11
  177.1 15.0 %collective-permute-start.4 = (bf16[640,1536]{1,0:T(8,128)(2,1)}, bf16[640,1536]{1,0:T(8,128)(2,1)}, u32[]{:S(2)}, u32[]{:S(2)}) collective-permute-start(bf16[640,1536]{1,0:T(8,128)(2,1)} %add_convert_fusion), channel_id=1, source_target_pairs={{0,1},{1,0},{2,3},{3,2},{4,5},{5,4},{6,7},{7,6},{8,9},{9,8},{10,11... | collective-permute-start | bytes 5898248 | tf_op jit(solution)/shard_map/ppermute | solution.py:456
  181.8 5.9 %copy-start.17 = (f32[1,640]{1,0:T(1,128)S(1)}, f32[1,640]{1,0:T(1,128)}, u32[]{:S(2)}) copy-start(f32[1,640]{1,0:T(1,128)} %get-tuple-element.34) | copy-start | bytes 7684
  181.8 6.5 %copy-start.7 = (bf16[640,384]{1,0:T(8,128)(2,1)S(1)}, bf16[640,384]{1,0:T(8,128)(2,1)}, u32[]{:S(2)}) copy-start(bf16[640,384]{1,0:T(8,128)(2,1)} %get-tuple-element.33.u2_ref) | copy-start | bytes 1474564
  181.8 30.9 %all-to-all-start.2 = ((bf16[64,8,1536]{2,1,0:T(8,128)(2,1)}), bf16[64,8,1536]{2,1,0:T(8,128)(2,1)}, u32[]{:S(2)}, u32[]{:S(2)}) async-start(bf16[64,8,1536]{2,1,0:T(8,128)(2,1)} %fusion.3), calls=%async_computation.2 | async-start | bytes 3145728 | tf_op jit(solution)/shard_map/all_to_all | solution.py:452
  187.8 1.8 copy-start.15
  187.8 1.8 copy-start.5
  187.8 1.8 copy-start.12
  187.8 4.3 %collective-permute-start.5 = (f32[1,1152]{1,0:T(1,128)S(1)}, f32[1,1152]{1,0:T(1,128)S(1)}, u32[]{:S(2)}, u32[]{:S(2)}) collective-permute-start(f32[1,1152]{1,0:T(1,128)S(1)} %pad_maximum_fusion.part_ref), channel_id=1, source_target_pairs={{0,1},{1,0},{2,3},{3,2},{4,5},{5,4},{6,7},{7,6},{8,9},{9,8},{10,11... | collective-permute-start | bytes 13832 | tf_op jit(solution)/shard_map/ppermute | solution.py:456
  192.1 0.6 copy-start.16
  197.7 20.3 %copy-start.13 = (s32[384,2]{0,1:T(2,128)S(1)}, s32[384,2]{0,1:T(2,128)}, u32[]{:S(2)}) copy-start(s32[384,2]{0,1:T(2,128)} %param.9) | copy-start | bytes 9220
  212.7 35.1 %all-to-all-start.4 = ((bf16[64,8,2048]{2,1,0:T(8,128)(2,1)}), bf16[64,8,2048]{2,1,0:T(8,128)(2,1)S(1)}, u32[]{:S(2)}, u32[]{:S(2)}) async-start(bf16[64,8,2048]{2,1,0:T(8,128)(2,1)} %pack.1), calls=%async_computation.4 | async-start | bytes 4194304 | tf_op jit(solution)/shard_map/all_to_all | solution.py:452
  221.3 11.3 %copy-start.9 = (bf16[1152,384]{1,0:T(8,128)(2,1)S(1)}, bf16[1152,384]{1,0:T(8,128)(2,1)}, u32[]{:S(2)}) copy-start(bf16[1152,384]{1,0:T(8,128)(2,1)} %get-tuple-element.31.refs_1_) | copy-start | bytes 2654212
  232.6 9.9 %collective-permute-start.6 = (f32[2,3072]{1,0:T(2,128)}, f32[2,3072]{1,0:T(2,128)S(1)}, u32[]{:S(2)}, u32[]{:S(2)}) collective-permute-start(f32[2,3072]{1,0:T(2,128)} %get-tuple-element.41), channel_id=1, source_target_pairs={{0,1},{1,0},{2,3},{3,2},{4,5},{5,4},{6,7},{7,6},{8,9},{9,8},{10,11... | collective-permute-start | bytes 73736 | tf_op jit(solution)/shard_map/ppermute | solution.py:456
  234.8 2.6 %copy-start.18 = (bf16[640,3072]{1,0:T(8,128)(2,1)S(1)}, bf16[640,3072]{1,0:T(8,128)(2,1)}, u32[]{:S(2)}) copy-start(bf16[640,3072]{1,0:T(8,128)(2,1)} %get-tuple-element.40) | copy-start | bytes 11796484
  237.4 5.1 %copy-start.14 = (f32[2,3072]{1,0:T(2,128)S(1)}, f32[2,3072]{1,0:T(2,128)}, u32[]{:S(2)}) copy-start(f32[2,3072]{1,0:T(2,128)} %get-tuple-element.41) | copy-start | bytes 73732
  247.9 1.4 copy-start

commit v2 on v1

--- a/solution.py
+++ b/solution.py
@@ -69,42 +69,19 @@
     return total
 
 
-def send_tokens_kernel(exp_ref, gate_ref, src_ref, out_ref, ranks_ref, gates_ref, line_ref, small_ref):
+def send_first_kernel(exp_ref, gate_ref, tok_ref, cot_ref, out_ref, ranks_ref, gates_ref, line_ref, small_ref):
     b = pl.program_id(0)
 
     @pl.when(b == 0)
     def _():
         exp = exp_ref[...]
+        first, second = named_by(exp)
         named, ranks = slot_ranks(exp)
         small = jnp.where(named > 0.5, ranks, -1.0).astype(BF)
         small_ref[...] = small
         ranks_ref[...] = spread_rows(small)
-        for k, mask in enumerate(named_by(exp)):
+        for k, mask in enumerate((first, second)):
             line_ref[k : k + 1, :] = jnp.sum(jnp.where(mask, ranks, 0.0), axis=0, keepdims=True)
-
-    def rows(piece, lo, hi):
-        hit = ones_where(ranks_ref[...] == row_slots(jnp.int32(piece))).astype(BF)
-        return dot(hit, src_ref[:, lo:hi]).reshape(E, 8, hi - lo).astype(BF)
-
-    @pl.when(b == 0)
-    def _():
-        out_ref[...] = rows(0, 0, 1152)
-
-    @pl.when(b == 1)
-    def _():
-        out_ref[:, :, 0:384] = rows(0, 1152, 1536)
-        out_ref[:, :, 384:1152] = rows(1, 0, 768)
-
-    @pl.when(b == 2)
-    def _():
-        out_ref[:, :, 0:768] = rows(1, 768, 1536)
-        row = iota((128, E), 0)
-        spread = ones_where(row // 2 == iota((128, E), 1)).astype(BF)
-        slot = (16 + iota((128, TOK), 0) % 2).astype(F32)
-        hit = ones_where(dot(spread, small_ref[...]) == slot).astype(BF)
-        last = dot(hit, src_ref[...]).astype(BF)
-        out_ref[:, :, 768:1152] = put_last(last).reshape(E, 8, Q).astype(BF)
-        first, second = named_by(exp_ref[...])
         gate = gate_ref[...]
         rest = jnp.where(first, gate[0:1, :], 0.0) + jnp.where(second, gate[1:2, :], 0.0)
         total = jnp.zeros((F1, TOK), F32)
@@ -114,25 +91,53 @@
             total = total + spread_rows(part)
         gates_ref[...] = total
 
-
-def send_tokens(exp_t, gate_t, tokens):
+    def rows(piece, lo, hi):
+        hit = ones_where(ranks_ref[...] == row_slots(jnp.int32(piece))).astype(BF)
+        return dot(hit, tok_ref[:, lo:hi]).reshape(E, 8, hi - lo).astype(BF)
+
+    @pl.when(b == 0)
+    def _():
+        hit = ranks_ref[...] == row_slots(jnp.int32(0))
+        scale = jnp.sum(jnp.where(hit, gates_ref[...], 0.0), axis=1, keepdims=True)
+        scaled = dot(ones_where(hit).astype(BF), cot_ref[...]) * scale
+        out_ref[:, :, 0:H] = scaled.reshape(E, 8, H).astype(BF)
+        out_ref[:, :, H:1664] = rows(0, 0, 128)
+
+    @pl.when(b == 1)
+    def _():
+        out_ref[:, :, 0:1408] = rows(0, 128, H)
+        out_ref[:, :, 1408:1664] = rows(1, 0, 256)
+
+    @pl.when(b == 2)
+    def _():
+        out_ref[:, :, 0:1280] = rows(1, 256, H)
+        row = iota((128, E), 0)
+        spread = ones_where(row // 2 == iota((128, E), 1)).astype(BF)
+        slot = (16 + iota((128, TOK), 0) % 2).astype(F32)
+        hit = ones_where(dot(spread, small_ref[...]) == slot).astype(BF)
+        last = dot(hit, tok_ref[...]).astype(BF)
+        out_ref[:, :, 1280:1664] = put_last(last).reshape(E, 8, Q).astype(BF)
+
+
+def send_first(exp_t, gate_t, tokens, cotangent):
     small = pl.BlockSpec((2, TOK), lambda b: (0, 0))
     table = pl.BlockSpec((F1, TOK), lambda b: (0, 0))
+    source = pl.BlockSpec((TOK, H), lambda b: (0, 0))
     shape = jax.ShapeDtypeStruct((F1, TOK), F32)
     return pl.pallas_call(
-        send_tokens_kernel,
+        send_first_kernel,
         grid=(3,),
-        in_specs=[small, small, pl.BlockSpec((TOK, H), lambda b: (0, 0))],
-        out_specs=[pl.BlockSpec((E, 8, 1152), lambda b: (0, 0, b)), table, table, small],
+        in_specs=[small, small, source, source],
+        out_specs=[pl.BlockSpec((E, 8, 1664), lambda b: (0, 0, b)), table, table, small],
         out_shape=[
-            jax.ShapeDtypeStruct((E, 8, 3456), BF),
+            jax.ShapeDtypeStruct((E, 8, 4992), BF),
             shape,
             shape,
             jax.ShapeDtypeStruct((2, TOK), F32),
         ],
         scratch_shapes=[pltpu.VMEM((E, TOK), BF)],
-        name="send_tokens",
-    )(exp_t, gate_t, tokens)
+        name="send_first",
+    )(exp_t, gate_t, tokens, cotangent)
 
 
 def send_kernel(lo, last, ranks_ref, gates_ref, src_ref, out_ref):
@@ -183,39 +188,42 @@
     return pieces
 
 
-def fill_rows(steps, core_ref, own_ref, other_ref, own_last_ref, other_last_ref, rows_ref):
+def fill_rows(steps, core_ref, parts, rows_ref):
     b = pl.program_id(0)
     core = core_ref[0]
-    sides = ((core, own_ref, own_last_ref), (1 - core, other_ref, other_last_ref))
+    halves = (core, 1 - core)
 
     @pl.when(b < steps)
     def _():
-        for half, part_ref, _ in sides:
+        for half, part_ref in zip(halves, parts[:2]):
             rows = part_ref[...].astype(F32).reshape(128, H).astype(BF)
             rows_ref[:, pl.ds(pl.multiple_of(half * H, H), H)] = rows
 
-    @pl.when(b == steps)
-    def _():
-        for half, _, last_ref in sides:
-            for q, piece in enumerate(unpack_last(last_ref[...])):
-                rows_ref[:, pl.ds(pl.multiple_of(half * H + q * Q, Q), Q)] = piece
-
-
-def packed_specs(wide):
+    if len(parts) == 4:
+
+        @pl.when(b == steps)
+        def _():
+            for half, last_ref in zip(halves, parts[2:]):
+                for q, piece in enumerate(unpack_last(last_ref[...])):
+                    rows_ref[:, pl.ds(pl.multiple_of(half * H + q * Q, Q), Q)] = piece
+
+
+def packed_specs(start, wide, last_at):
     steps = 4 * wide
 
     def rows_at(b):
         bb = jnp.minimum(b, steps - 1)
-        return (bb % 4, 0, bb // 4)
+        return (bb % 4, 0, start + bb // 4)
 
     rows = pl.BlockSpec((16, 8, H), rows_at)
-    last = pl.BlockSpec((E, 8, Q), lambda b: (0, 0, wide * 4))
-    return [pl.BlockSpec(memory_space=pltpu.SMEM), rows, rows, last, last]
+    last = pl.BlockSpec((E, 8, Q), lambda b: (0, 0, last_at))
+    specs = [pl.BlockSpec(memory_space=pltpu.SMEM), rows, rows]
+    return specs + [last, last] if last_at else specs
 
 
 def forward_kernel(core_ref, own_ref, other_ref, own_last_ref, other_last_ref, *refs):
     gate_ref, up_ref, rows_ref, hidden_ref, active_ref, slope_ref = refs
-    fill_rows(8, core_ref, own_ref, other_ref, own_last_ref, other_last_ref, rows_ref)
+    fill_rows(8, core_ref, (own_ref, other_ref, own_last_ref, other_last_ref), rows_ref)
     rows = rows_ref[...]
     gate_pre = dot(rows, gate_ref[...])
     up_pre = dot(rows, up_ref[...])
@@ -232,7 +240,7 @@
     return pl.pallas_call(
         forward_kernel,
         grid=(9,),
-        in_specs=packed_specs(2) + [weights, weights],
+        in_specs=packed_specs(1, 2, 12) + [weights, weights],
         out_specs=[pl.BlockSpec((128, 2 * H), lambda b: (b, 0)), block, block, block],
         out_shape=[
             jax.ShapeDtypeStruct((1152, 2 * H), BF),
@@ -244,38 +252,53 @@
     )(core, own, other, own, other, gate_mat, up_mat)
 
 
-def middle_kernel(core_ref, own_ref, other_ref, own_last_ref, other_last_ref, *refs):
-    down_ref, hidden_ref, active_ref, slope_ref, rows_ref, gate_ref, up_ref, part_ref = refs
-    fill_rows(4, core_ref, own_ref, other_ref, own_last_ref, other_last_ref, rows_ref)
+def middle_kernel(core_ref, *refs):
+    down_ref, back_ref, hidden_ref, active_ref, slope_ref = refs[-10:-5]
+    rows_ref, gate_ref, up_ref, part_ref, sent_ref = refs[-5:]
+    fill_rows(4, core_ref, refs[:-10], rows_ref)
     grad = dot(rows_ref[...], down_ref[...])
     part = jnp.sum(hidden_ref[...].astype(F32) * grad, axis=1, keepdims=True)
     part_ref[...] = jnp.broadcast_to(part, (128, 128)).T[0:1, :]
-    gate_ref[...] = (grad * slope_ref[...]).astype(BF)
-    up_ref[...] = (grad * active_ref[...]).astype(BF)
-
-
-def middle(core, own, other, down_turned, hidden, active, slope):
-    late = pl.BlockSpec((128, Q), lambda b: (b + 4, 0))
+    gate = (grad * slope_ref[...]).astype(BF)
+    up = (grad * active_ref[...]).astype(BF)
+    gate_ref[...] = gate
+    up_ref[...] = up
+    sent_ref[...] = dot(jnp.concatenate([gate, up], axis=1), back_ref[...]).astype(BF)
+
+
+def middle(core, own, other, down_turned, back_turned, hidden, active, slope, lo, last):
+    taken = pl.BlockSpec((128, Q), lambda b: (b + lo, 0))
     block = pl.BlockSpec((128, Q), lambda b: (b, 0))
-    shape = jax.ShapeDtypeStruct((640, Q), BF)
+    steps = 5 if last else 4
+    shape = jax.ShapeDtypeStruct((128 * steps, Q), BF)
+    sides = (own, other, own, other) if last else (own, other)
     return pl.pallas_call(
         middle_kernel,
-        grid=(5,),
-        in_specs=packed_specs(1) + [pl.BlockSpec((2 * H, Q), lambda b: (0, 0)), late, late, late],
+        grid=(steps,),
+        in_specs=packed_specs(0, 1, 4 if last else 0)
+        + [
+            pl.BlockSpec((2 * H, Q), lambda b: (0, 0)),
+            pl.BlockSpec((2 * Q, H), lambda b: (0, 0)),
+            taken,
+            taken,
+            taken,
+        ],
         out_specs=[
             pl.BlockSpec((128, 2 * H), lambda b: (b, 0)),
             block,
             block,
             pl.BlockSpec((1, 128), lambda b: (0, b)),
+            pl.BlockSpec((128, H), lambda b: (b, 0)),
         ],
         out_shape=[
-            jax.ShapeDtypeStruct((640, 2 * H), BF),
+            jax.ShapeDtypeStruct((128 * steps, 2 * H), BF),
             shape,
             shape,
-            jax.ShapeDtypeStruct((1, 640), F32),
+            jax.ShapeDtypeStruct((1, 128 * steps), F32),
+            jax.ShapeDtypeStruct((128 * steps, H), BF),
         ],
         name="middle",
-    )(core, own, other, own, other, down_turned, hidden, active, slope)
+    )(core, *sides, down_turned, back_turned, hidden, active, slope)
 
 
 def pack_kernel(mine_ref, got_ref, mine_last_ref, got_last_ref, part_ref, got_part_ref, out_ref):
@@ -402,6 +425,39 @@
     )(ranks, lines, exp_t, gate_t, total, two, two, two)
 
 
+def down_grads_kernel(hidden_ref, one_ref, two_ref, out_ref, norm_ref, turned_ref, sums_ref):
+    b = pl.program_id(0)
+
+    @pl.when(b == 0)
+    def _():
+        turned_ref[...] = hidden_ref[...].T
+        sums_ref[...] = jnp.zeros((Q, 128), F32)
+
+    total = dot(turned_ref[:, 0:F1], one_ref[...]) + dot(turned_ref[:, F1:1152], two_ref[...])
+    out_ref[...] = total.astype(BF)
+    sums_ref[...] += jnp.broadcast_to(jnp.sum(total * total, axis=1, keepdims=True), (Q, 128))
+
+    @pl.when(b == 5)
+    def _():
+        norm_ref[...] = sums_ref[...].T[0:1, :]
+
+
+def down_grads(hidden, one, two):
+    return pl.pallas_call(
+        down_grads_kernel,
+        grid=(6,),
+        in_specs=[
+            pl.BlockSpec((1152, Q), lambda b: (0, 0)),
+            pl.BlockSpec((F1, 512), lambda b: (0, b)),
+            pl.BlockSpec((640, 512), lambda b: (0, b)),
+        ],
+        out_specs=[pl.BlockSpec((Q, 512), lambda b: (0, b)), pl.BlockSpec((1, Q), lambda b: (0, 0))],
+        out_shape=[jax.ShapeDtypeStruct((Q, 2 * H), BF), jax.ShapeDtypeStruct((1, Q), F32)],
+        scratch_shapes=[pltpu.VMEM((Q, 1152), BF), pltpu.VMEM((Q, 128), F32)],
+        name="down_grads",
+    )(hidden, one, two)
+
+
 def turn_kernel(src_ref, out_ref):
     out_ref[...] = src_ref[...].T
 
@@ -415,6 +471,26 @@
         out_shape=jax.ShapeDtypeStruct((2 * H, Q), BF),
         name="turn",
     )(mat)
+
+
+def turn_back_kernel(core_ref, gate_ref, up_ref, out_ref):
+    out_ref[0:Q, :] = gate_ref[...].T
+    out_ref[Q : 2 * Q, :] = up_ref[...].T
+
+
+def turn_back(core, gate_mat, up_mat):
+    block = pl.BlockSpec((512, Q), lambda b, c: (3 * (1 - c[0]) + b, 0))
+    return pl.pallas_call(
+        turn_back_kernel,
+        grid_spec=pltpu.PrefetchScalarGridSpec(
+            num_scalar_prefetch=1,
+            grid=(3,),
+            in_specs=[block, block],
+            out_specs=pl.BlockSpec((2 * Q, 512), lambda b, c: (0, b)),
+        ),
+        out_shape=jax.ShapeDtypeStruct((2 * Q, H), BF),
+        name="turn_back",
+    )(core, gate_mat, up_mat)
 
 
 def weight_grads_kernel(x_ref, g1_ref, u1_ref, g2_ref, u2_ref, gate_ref, up_ref, norm_ref, turned_ref):
@@ -465,60 +541,42 @@
     core_arg = core.reshape(1)
     gate_mat, up_mat, down_mat = w_gate[0], w_up[0], w_down[0]
     exp_t, gate_t = experts.T, gate.T
-    gates = [half(gate_mat, index, 0) for index in (core, 1 - core)]
-    ups = [half(up_mat, index, 0) for index in (core, 1 - core)]
-    downs = [half(down_mat, index, 1) for index in (core, 1 - core)]
+    gate_half, up_half = half(gate_mat, core, 0), half(up_mat, core, 0)
     down_turned = turn(down_mat)
-    tok_own, ranks, gates_of, lines = send_tokens(exp_t, gate_t, tokens)
-    tok_own = to_experts(tok_own)
-    cot_one = send(ranks, gates_of, cotangent, 0, 4)
-    cot_one = to_experts(cot_one)
+    back_turned = turn_back(core_arg, gate_mat, up_mat)
+    own, ranks, gates_of, lines = send_first(exp_t, gate_t, tokens, cotangent)
+    own = to_experts(own)
     cot_two = send(ranks, gates_of, cotangent, 4, 9)
     by_token = token_ranks(experts)
     cot_two = to_experts(cot_two)
-    tok_other = swap_cores(tok_own)
-
-    rows_in, hidden, active, gate_slope = forward(core_arg, tok_own, tok_other, gate_mat, up_mat)
-
-    def send_back(gate_grad_pre, up_grad_pre):
-        def partial(index):
-            return (dot_last(gate_grad_pre, gates[index]) + dot_last(up_grad_pre, ups[index])).astype(BF)
-
-        sent = swap_cores(partial(1))
-        return partial(0), sent
-
-    cot_one_other = swap_cores(cot_one)
-    own = cot_one.reshape(F1, H)
-    other = cot_one_other.reshape(F1, H)
-    grad = dot_last(own, downs[0]) + dot_last(other, downs[1])
-    parts_one = jnp.sum(hidden[:F1].astype(F32) * grad, axis=1)
-    gate_one = (grad * gate_slope[:F1]).astype(BF)
-    up_one = (grad * active[:F1]).astype(BF)
-    mine, sent = send_back(gate_one, up_one)
-    back_one = (mine.astype(F32) + sent.astype(F32)).astype(BF).reshape(E, 8, H)
+    other = swap_cores(own)
+
+    rows_in, *terms = forward(core_arg, own, other, gate_mat, up_mat)
+
+    def kept(gate_grad_pre, up_grad_pre):
+        return (dot_last(gate_grad_pre, gate_half) + dot_last(up_grad_pre, up_half)).astype(BF)
+
+    rows_one, gate_one, up_one, parts_one, sent = middle(
+        core_arg, own, other, down_turned, back_turned, *terms, 0, False
+    )
+    sent = swap_cores(sent)
+    back_one = kept(gate_one, up_one).astype(F32) + sent.astype(F32)
+    back_one = back_one.astype(BF).reshape(E, 8, H)
     back_one = to_experts(back_one)
 
     cot_two_other = swap_cores(cot_two)
-    rows_two, gate_two, up_two, parts_two = middle(
-        core_arg, cot_two, cot_two_other, down_turned, hidden, active, gate_slope
+    rows_two, gate_two, up_two, parts_two, sent = middle(
+        core_arg, cot_two, cot_two_other, down_turned, back_turned, *terms, 4, True
     )
-    mine, sent = send_back(gate_two, up_two)
-    parts = jnp.concatenate([parts_one.reshape(1, F1), parts_two], axis=1)
+    sent = swap_cores(sent)
+    mine = kept(gate_two, up_two)
+    parts = jnp.concatenate([parts_one, parts_two], axis=1)
     back_two = pack(mine, sent, parts, swap_cores(parts))
     back_two = to_experts(back_two)
 
-    down_own = dot_rows(hidden[:F1], own)
-    down_other = dot_rows(hidden[:F1], other)
     gate_grad, up_grad, norms = weight_grads(rows_in, gate_one, up_one, gate_two, up_two)
     norms = norms + swap_cores(norms)
-    down_one = jnp.where(
-        core == 0,
-        jnp.concatenate([down_own, down_other], axis=1),
-        jnp.concatenate([down_other, down_own], axis=1),
-    )
-    down_sum = down_one + dot_rows(hidden[F1:], rows_two)
-    down_norms = jnp.sum(down_sum * down_sum, axis=1)
-
+    down_grad, down_norms = down_grads(terms[0], rows_one, rows_two)
     back_sum = combine_one(by_token, back_one)
     token_grad, gates_grad = combine_two(by_token, lines, exp_t, gate_t, back_sum, back_two)
     return (
@@ -526,10 +584,10 @@
         gates_grad.T,
         gate_grad[None],
         up_grad[None],
-        down_sum.astype(BF)[None],
+        down_grad[None],
         norms[0:1],
         norms[1:2],
-        down_norms[None],
+        down_norms,
     )
 
 

time: 257 us -> 248 us (0.965)
  blocking collectives: 0 us -> 109 us
  waiting for transfers between devices: 104 us -> 17.2 us
  matrix products: 32.7 us -> 5.72 us
  starting transfers between devices: 37.6 us -> 12.2 us
  Pallas kernels: 74.9 us -> 93.9 us
  other arithmetic: 0.02 us -> 2.95 us
    all_to_all x0 -> x2, blocking collectives: none -> 109 us  [to_experts(): return lax.all_to_all(x, 'ep', split_axis=0, concat_axis=0, tiled=True)]
    all_to_all x5 -> x2, waiting for transfers between devices: 104 us -> 17.2 us  [to_experts(): return lax.all_to_all(x, 'ep', split_axis=0, concat_axis=0, tiled=True)]
    all_to_all x5 -> x2, starting transfers between devices: 36.3 us -> 11.2 us  [to_experts(): return lax.all_to_all(x, 'ep', split_axis=0, concat_axis=0, tiled=True)]
    pallas_call x3 -> x6, Pallas kernels: 31 us -> 54.7 us  [the longest x2 18.9 us: middle(): pl.pallas_call(middle_kernel, grid=(steps,), in_specs=packed_specs(0, 1,...]
    dot_general x10 -> x4, matrix products: 23.6 us -> 5.72 us  [dot_last(): lax.dot_general(a, b, (((1,), (1,)), ((), ())), preferred_element_type=F32)]
    dot_general x3 -> x0, matrix products: 9.07 us -> none  [dot_rows(): lax.dot_general(a, b, (((0,), (0,)), ((), ())), preferred_element_type=F32)]
    pallas_call x2 -> x1, Pallas kernels: 10.6 us -> 5.97 us  [send(): pl.pallas_call(functools.partial(send_kernel, lo, hi == 9), grid=(hi - lo...]
    reshape x0 -> x1, other arithmetic: none -> 2.93 us  [step(): back_one = back_one.astype(BF).reshape(E, 8, H)]
  transfers between devices with their start and end apart: 12 -> 8, of which waited for: 5 -> 2; matrix products, arithmetic and copies ran while one was open for 14% -> 4% of each run, Pallas kernels for 20% -> 30%
where the time goes in v2:
time: 248 us; the launch traced here: 247 us
  blocking collectives  109 us (44%)
  Pallas kernels  93.9 us (38%)
  waiting for transfers between devices  17.2 us (7%)
  starting transfers between devices  12.2 us (5%)
  matrix products  5.72 us (2%)
  local copies, waits for them, and re-layouts  4.62 us (2%)
  other arithmetic  2.95 us (1%)
    all_to_all x2, blocking collectives, to_experts(): return lax.all_to_all(x, 'ep', split_axis=0, concat_axis=0, tiled=True)  109 us
    pallas_call x2, Pallas kernels, middle(): pl.pallas_call(middle_kernel, grid=(steps,), in_specs=packed_specs(0, 1,...  18.9 us
    all_to_all x2, waiting for transfers between devices, to_experts(): return lax.all_to_all(x, 'ep', split_axis=0, concat_axis=0, tiled=True)  17.2 us
    pallas_call x1, Pallas kernels, forward(): pl.pallas_call(forward_kernel, grid=(9,), in_specs=packed_specs(1, 2, 12)...  14.8 us
    pallas_call x1, Pallas kernels, weight_grads(): pl.pallas_call(weight_grads_kernel, grid=(6,), in_specs=[pl.BlockSpec((11...  11.2 us
    all_to_all x2, starting transfers between devices, to_experts(): return lax.all_to_all(x, 'ep', split_axis=0, concat_axis=0, tiled=True)  11.2 us
    pallas_call x1, Pallas kernels, down_grads(): pl.pallas_call(down_grads_kernel, grid=(6,), in_specs=[pl.BlockSpec((1152...  8.86 us
    pallas_call x1, Pallas kernels, send_first(): pl.pallas_call(send_first_kernel, grid=(3,), in_specs=[small, small, sour...  7.95 us
  transfers between devices with their start and end apart: 8, of which 2 were waited for; matrix products, arithmetic and copies ran while one was open for 4% of the time, Pallas kernels for 30%

profile of v2, /device:TPU:0, one launch (start us, length us, event | category | flops | bytes accessed | tf_op | source)
XLA Modules:
  0.0 246.7 jit_solution(8665100749803325678)
XLA Ops:
  0.6 7.9 %send_first.1 = (bf16[64,8,4992]{2,1,0:T(8,128)(2,1)}, f32[512,384]{1,0:T(8,128)}, f32[512,384]{1,0:T(8,128)}, f32[2,384]{1,0:T(2,128)}) custom-call(s32[2,384]{1,0:T(2,128)} %bitcast.31, f32[2,384]{1,0:T(2,128)} %bitcast.33, bf16[384,1536]{1,0:T(8,128)(2,1)} %tok_ref.1, bf16[384,1536]{1,0:T(8,128)(2,1)} %src_ref.1), custom_call_target="tpu_custom_call" | custom-call | tf_op jit(solution)/shard_map/send_first/pallas_call | solution.py:127
  8.6 74.1 %all_to_all.20.own_ref.own_last_ref.refs_0_ = bf16[64,8,4992]{2,1,0:T(8,128)(2,1)} all-to-all(bf16[64,8,4992]{2,1,0:T(8,128)(2,1)} %get-tuple-element.34), channel_id=1, replica_groups=mesh['ep'=64,'tp'=2] {'ep'}, dimensions={0} | all-to-all | bytes 10223616 | tf_op jit(solution)/shard_map/all_to_all | solution.py:528
  82.7 0.0 collective-permute-start
  82.7 6.0 %send.1 = bf16[64,8,1920]{2,1,0:T(8,128)(2,1)} custom-call(f32[512,384]{1,0:T(8,128)} %get-tuple-element.41.ranks_ref, f32[512,384]{1,0:T(8,128)} %get-tuple-element.42.gates_ref, bf16[384,1536]{1,0:T(8,128)(2,1)} %src_ref.1), custom_call_target="tpu_custom_call" | custom-call | tf_op jit(solution)/shard_map/send/pallas_call | solution.py:171
  88.6 35.2 %all_to_all.21.refs_0_.refs_2_ = bf16[64,8,1920]{2,1,0:T(8,128)(2,1)} all-to-all(bf16[64,8,1920]{2,1,0:T(8,128)(2,1)} %send.1), channel_id=1, replica_groups=mesh['ep'=64,'tp'=2] {'ep'}, dimensions={0} | all-to-all | bytes 3932160 | tf_op jit(solution)/shard_map/all_to_all | solution.py:528
  123.8 0.0 collective-permute-start.2
  123.8 5.3 %turn.1.refs_2_.refs_4_ = bf16[3072,384]{1,0:T(8,128)(2,1)} custom-call(bf16[384,3072]{1,0:T(8,128)(2,1)} %bitcast.30), custom_call_target="tpu_custom_call" | custom-call | tf_op jit(solution)/shard_map/turn/pallas_call | solution.py:466
  129.1 4.2 %turn_back.1.refs_3_.refs_5_ = bf16[768,1536]{1,0:T(8,128)(2,1)} custom-call(s32[1]{0:T(128)} %bitcast.2.core_ref, bf16[3072,384]{1,0:T(8,128)(2,1)} %bitcast.28, bf16[3072,384]{1,0:T(8,128)(2,1)} %bitcast.26), custom_call_target="tpu_custom_call" | custom-call | tf_op jit(solution)/shard_map/turn_back/pallas_call | solution.py:483
  133.3 0.0 collective-permute-done.other_ref.other_last_ref.refs_1_
  133.3 14.8 %forward.1 = (bf16[1152,3072]{1,0:T(8,128)(2,1)}, bf16[1152,384]{1,0:T(8,128)(2,1)}, f32[1152,384]{1,0:T(8,128)}, f32[1152,384]{1,0:T(8,128)}) custom-call(s32[1]{0:T(128)} %bitcast.2.core_ref, bf16[64,8,4992]{2,1,0:T(8,128)(2,1)} %all_to_all.20.own_ref.own_last_ref.refs_0_, bf16[64,8,4992]{2,1,0:T(8,128)(2,1)} %collective-permute-done.other_ref.other_last_ref.refs_1_, ...), custom_call_target="tpu_custom_call" | custom-call | tf_op jit(solution)/shard_map/forward/pallas_call | solution.py:240
  148.1 8.4 %middle.2 = (bf16[512,3072]{1,0:T(8,128)(2,1)}, bf16[512,384]{1,0:T(8,128)(2,1)}, bf16[512,384]{1,0:T(8,128)(2,1)}, f32[1,512]{1,0:T(1,128)}, bf16[512,1536]{1,0:T(8,128)(2,1)}) custom-call(s32[1]{0:T(128)} %bitcast.2.core_ref, bf16[64,8,4992]{2,1,0:T(8,128)(2,1)} %all_to_all.20.own_ref.own_last_ref.refs_0_, ...), custom_call_target="tpu_custom_call" | custom-call | tf_op jit(solution)/shard_map/middle/pallas_call | solution.py:275
  156.5 0.7 collective-permute-start.1
  157.1 0.0 copy-start.1
  157.1 0.0 copy-start.5
  157.2 0.0 collective-permute-done.2.refs_1_.refs_3_
  157.2 10.5 %middle.3 = (bf16[640,3072]{1,0:T(8,128)(2,1)}, bf16[640,384]{1,0:T(8,128)(2,1)}, bf16[640,384]{1,0:T(8,128)(2,1)}, f32[1,640]{1,0:T(1,128)}, bf16[640,1536]{1,0:T(8,128)(2,1)}) custom-call(s32[1]{0:T(128)} %bitcast.2.core_ref, bf16[64,8,1920]{2,1,0:T(8,128)(2,1)} %all_to_all.21.refs_0_.refs_2_, bf16[64,8,1920]{2,1,0:T(8,128)(2,1)} %collective-permute-done.2.refs_1_.refs_3_, ...), custom_call_target="tpu_custom_call" | custom-call | tf_op jit(solution)/shard_map/middle/pallas_call | solution.py:275
  167.7 0.1 collective-permute-start.3
  167.8 0.0 copy-done.1
  167.8 0.0 copy-done.5
  167.8 0.0 copy-start.2
  167.8 0.0 copy-start.7
  167.8 1.0 fusion.4
  168.8 0.6 copy-done.2
  169.5 0.0 copy-done.7
  169.5 1.0 fusion
  170.5 0.0 collective-permute-done.1
  170.5 2.9 %fusion.1 = bf16[64,8,1536]{2,1,0:T(8,128)(2,1)} fusion(bf16[512,1536]{1,0:T(8,128)(2,1)} %collective-permute-done.1, bf16[512,1536]{1,0:T(8,128)(2,1)S(1)} %fusion), kind=kLoop, calls=%fused_computation.4 | loop fusion | flops 3145728 | bytes 4718592 | tf_op jit(solution)/shard_map/reshape | solution.py:564
  173.4 0.0 copy-start.13
  173.5 0.0 copy-start.12
  173.5 0.0 copy-start.4
  173.5 5.9 %all-to-all-start.1 = ((bf16[64,8,1536]{2,1,0:T(8,128)(2,1)}), bf16[64,8,1536]{2,1,0:T(8,128)(2,1)}, u32[]{:S(2)}, u32[]{:S(2)}) async-start(bf16[64,8,1536]{2,1,0:T(8,128)(2,1)} %fusion.1), calls=%async_computation.1 | async-start | bytes 3145728 | tf_op jit(solution)/shard_map/all_to_all | solution.py:528
  179.4 0.0 copy-done.13
  179.4 0.0 copy-done.12
  179.4 0.0 copy-start.10
  179.4 0.3 collective-permute-start.4
  179.7 0.0 copy-done.4
  179.7 0.0 copy-start.3
  179.7 0.0 copy-start.6
  179.7 1.2 fusion.2
  180.9 0.0 copy-done.10
  180.9 0.4 copy-done.3
  181.4 0.1 copy-done.6
  181.4 2.5 %add_convert_fusion.mine_ref.mine_last_ref = bf16[640,1536]{1,0:T(8,128)(2,1)} fusion(f32[640,1536]{1,0:T(8,128)S(1)} %fusion.2, bf16[640,384]{1,0:T(8,128)(2,1)S(1)} %copy-done.6, bf16[1,3072,384]{2,1,0:T(8,128)(2,1)S(1)} %copy-done.3, s32[]{:T(128)S(6)} %select_n.4), kind=kOutput, calls=%fused_computation | convolution fusion | flops 756940800 | bytes 7569412 | tf_op jit(solution)/shard_map/dot_general | solution.py:29
  183.9 0.0 collective-permute-done.4.got_part_ref
  183.9 0.0 copy-start.11
  183.9 0.0 collective-permute-done.3.got_ref.got_last_ref
  183.9 0.6 copy-done.11
  184.5 5.0 %pack.1 = bf16[64,8,2048]{2,1,0:T(8,128)(2,1)} custom-call(bf16[640,1536]{1,0:T(8,128)(2,1)} %add_convert_fusion.mine_ref.mine_last_ref, bf16[640,1536]{1,0:T(8,128)(2,1)} %collective-permute-done.3.got_ref.got_last_ref, bf16[640,1536]{1,0:T(8,128)(2,1)} %add_convert_fusion.mine_ref.mine_last_ref, ...), custom_call_target="tpu_custom_call" | custom-call | tf_op jit(solution)/shard_map/pack/pallas_call | solution.py:331
  189.6 14.7 %all-to-all-done.1.one_ref = bf16[64,8,1536]{2,1,0:T(8,128)(2,1)} async-done(((bf16[64,8,1536]{2,1,0:T(8,128)(2,1)}), bf16[64,8,1536]{2,1,0:T(8,128)(2,1)}, u32[]{:S(2)}, u32[]{:S(2)}) %all-to-all-start.1) | async-done | bytes 1572896 | tf_op jit(solution)/shard_map/all_to_all | solution.py:528
  204.3 5.3 %all-to-all-start.3 = ((bf16[64,8,2048]{2,1,0:T(8,128)(2,1)}), bf16[64,8,2048]{2,1,0:T(8,128)(2,1)S(1)}, u32[]{:S(2)}, u32[]{:S(2)}) async-start(bf16[64,8,2048]{2,1,0:T(8,128)(2,1)} %pack.1), calls=%async_computation.3 | async-start | bytes 4194304 | tf_op jit(solution)/shard_map/all_to_all | solution.py:528
  209.6 0.0 copy-start.8
  209.6 11.2 %weight_grads.1 = (bf16[3072,384]{1,0:T(8,128)(2,1)}, bf16[3072,384]{1,0:T(8,128)(2,1)}, f32[2,3072]{1,0:T(2,128)}) custom-call(bf16[1152,3072]{1,0:T(8,128)(2,1)} %get-tuple-element.50.x_ref, bf16[512,384]{1,0:T(8,128)(2,1)} %get-tuple-element.38.g1_ref, bf16[512,384]{1,0:T(8,128)(2,1)} %get-tuple-element.39.u1_ref, ...), custom_call_target="tpu_custom_call" | custom-call | tf_op jit(solution)/shard_map/weight_grads/pallas_call | solution.py:516
  220.8 0.0 collective-permute-start.5
  220.8 0.0 copy-done.8
  220.9 0.8 copy.15.exp_ref
  221.7 2.4 token_ranks.1.ranks_ref
  224.1 8.9 %down_grads.1 = (bf16[384,3072]{1,0:T(8,128)(2,1)}, f32[1,384]{1,0:T(1,128)}) custom-call(bf16[1152,384]{1,0:T(8,128)(2,1)} %get-tuple-element.35.refs_4_.refs_6_.hidden_ref, bf16[512,3072]{1,0:T(8,128)(2,1)} %get-tuple-element.53.one_ref, bf16[640,3072]{1,0:T(8,128)(2,1)} %get-tuple-element.54.two_ref), custom_call_target="tpu_custom_call" | custom-call | tf_op jit(solution)/shard_map/down_grads/pallas_call | solution.py:446
  233.0 0.0 collective-permute-done.5
  233.0 0.0 copy-done.9
  233.0 0.6 fusion.16
  233.6 3.4 %combine_one.1.refs_0_ = f32[384,1536]{1,0:T(8,128)} custom-call(f32[384,512]{1,0:T(8,128)} %token_ranks.1.ranks_ref, bf16[64,8,1536]{2,1,0:T(8,128)(2,1)} %all-to-all-done.1.one_ref), custom_call_target="tpu_custom_call" | custom-call | tf_op jit(solution)/shard_map/combine_one/pallas_call | solution.py:372
  237.0 2.4 all-to-all-done.3.refs_1_.refs_2_.refs_3_
  239.4 1.3 copy-done
  240.8 5.9 %combine_two.1 = (bf16[384,1536]{1,0:T(8,128)(2,1)}, f32[2,384]{1,0:T(2,128)}) custom-call(f32[384,512]{1,0:T(8,128)} %token_ranks.1.ranks_ref, f32[2,384]{1,0:T(2,128)} %get-tuple-element.33.line_ref, s32[2,384]{1,0:T(2,128)} %bitcast.32, f32[2,384]{1,0:T(2,128)} %bitcast.34, f32[384,1536]{1,0:T(8,128)} %combine_one.1.refs_0_, ...), custom_call_target="tpu_custom_call" | custom-call | tf_op jit(solution)/shard_map/combine_two/pallas_call | solution.py:409
  (5 shorter events, 0.0 us)
Async XLA Ops:
  82.7 50.6 %collective-permute-start = (bf16[64,8,4992]{2,1,0:T(8,128)(2,1)}, bf16[64,8,4992]{2,1,0:T(8,128)(2,1)}, u32[]{:S(2)}, u32[]{:S(2)}) collective-permute-start(bf16[64,8,4992]{2,1,0:T(8,128)(2,1)} %all_to_all.20.own_ref.own_last_ref.refs_0_), channel_id=1, source_target_pairs={{0,1},{1,0},{2,3},{3,2},{4,5},{5,4},{6,7},{7,6},{8,9},{9,8},{10,11... | collective-permute-start | bytes 15335432 | tf_op jit(solution)/shard_map/ppermute | solution.py:532
  123.8 33.3 %collective-permute-start.2 = (bf16[64,8,1920]{2,1,0:T(8,128)(2,1)}, bf16[64,8,1920]{2,1,0:T(8,128)(2,1)}, u32[]{:S(2)}, u32[]{:S(2)}) collective-permute-start(bf16[64,8,1920]{2,1,0:T(8,128)(2,1)} %all_to_all.21.refs_0_.refs_2_), channel_id=1, source_target_pairs={{0,1},{1,0},{2,3},{3,2},{4,5},{5,4},{6,7},{7,6},{8,9},{9,8},{10,11... | collective-permute-start | bytes 5898248 | tf_op jit(solution)/shard_map/ppermute | solution.py:532
  156.5 14.0 %collective-permute-start.1 = (bf16[512,1536]{1,0:T(8,128)(2,1)}, bf16[512,1536]{1,0:T(8,128)(2,1)}, u32[]{:S(2)}, u32[]{:S(2)}) collective-permute-start(bf16[512,1536]{1,0:T(8,128)(2,1)} %get-tuple-element.40), channel_id=1, source_target_pairs={{0,1},{1,0},{2,3},{3,2},{4,5},{5,4},{6,7},{7,6},{8,9},{9,8},{10,11... | collective-permute-start | bytes 4718600 | tf_op jit(solution)/shard_map/ppermute | solution.py:532
  157.1 10.6 %copy-start.1 = (bf16[1,3072,384]{2,1,0:T(8,128)(2,1)S(1)}, bf16[1,3072,384]{2,1,0:T(8,128)(2,1)}, u32[]{:S(2)}) copy-start(bf16[1,3072,384]{2,1,0:T(8,128)(2,1)} %param.12) | copy-start | bytes 7077892
  157.1 10.6 %copy-start.5 = (bf16[512,384]{1,0:T(8,128)(2,1)S(1)}, bf16[512,384]{1,0:T(8,128)(2,1)}, u32[]{:S(2)}) copy-start(bf16[512,384]{1,0:T(8,128)(2,1)} %get-tuple-element.39.u1_ref) | copy-start | bytes 1179652
  167.7 16.2 %collective-permute-start.3 = (bf16[640,1536]{1,0:T(8,128)(2,1)}, bf16[640,1536]{1,0:T(8,128)(2,1)}, u32[]{:S(2)}, u32[]{:S(2)}) collective-permute-start(bf16[640,1536]{1,0:T(8,128)(2,1)} %get-tuple-element.45), channel_id=1, source_target_pairs={{0,1},{1,0},{2,3},{3,2},{4,5},{5,4},{6,7},{7,6},{8,9},{9,8},{10,11... | collective-permute-start | bytes 5898248 | tf_op jit(solution)/shard_map/ppermute | solution.py:532
  167.8 1.7 copy-start.2
  167.8 1.7 copy-start.7
  173.4 5.9 %copy-start.13 = (f32[1,512]{1,0:T(1,128)S(1)}, f32[1,512]{1,0:T(1,128)}, u32[]{:S(2)}) copy-start(f32[1,512]{1,0:T(1,128)} %get-tuple-element.46) | copy-start | bytes 6148
  173.5 5.9 %copy-start.12 = (f32[1,640]{1,0:T(1,128)S(1)}, f32[1,640]{1,0:T(1,128)}, u32[]{:S(2)}) copy-start(f32[1,640]{1,0:T(1,128)} %get-tuple-element.47) | copy-start | bytes 7684
  173.5 6.2 %copy-start.4 = (bf16[640,384]{1,0:T(8,128)(2,1)S(1)}, bf16[640,384]{1,0:T(8,128)(2,1)}, u32[]{:S(2)}) copy-start(bf16[640,384]{1,0:T(8,128)(2,1)} %get-tuple-element.44.u2_ref) | copy-start | bytes 1474564
  173.5 30.8 %all-to-all-start.1 = ((bf16[64,8,1536]{2,1,0:T(8,128)(2,1)}), bf16[64,8,1536]{2,1,0:T(8,128)(2,1)}, u32[]{:S(2)}, u32[]{:S(2)}) async-start(bf16[64,8,1536]{2,1,0:T(8,128)(2,1)} %fusion.1), calls=%async_computation.1 | async-start | bytes 3145728 | tf_op jit(solution)/shard_map/all_to_all | solution.py:528
  179.4 1.5 copy-start.10
  179.4 4.5 %collective-permute-start.4 = (f32[1,1152]{1,0:T(1,128)S(1)}, f32[1,1152]{1,0:T(1,128)S(1)}, u32[]{:S(2)}, u32[]{:S(2)}) collective-permute-start(f32[1,1152]{1,0:T(1,128)S(1)} %constant_dynamic-update-slice_fusion.part_ref), channel_id=1, source_target_pairs={{0,1},{1,0},{2,3},{3,2},{4,5},{5,4},{6,7},{7,6},{8,9},{9,8},{10,11... | collective-permute-start | bytes 13832 | tf_op jit(solution)/shard_map/ppermute | solution.py:532
  179.7 1.7 copy-start.3
  179.7 1.7 copy-start.6
  183.9 0.6 copy-start.11
  204.3 35.2 %all-to-all-start.3 = ((bf16[64,8,2048]{2,1,0:T(8,128)(2,1)}), bf16[64,8,2048]{2,1,0:T(8,128)(2,1)S(1)}, u32[]{:S(2)}, u32[]{:S(2)}) async-start(bf16[64,8,2048]{2,1,0:T(8,128)(2,1)} %pack.1), calls=%async_computation.3 | async-start | bytes 4194304 | tf_op jit(solution)/shard_map/all_to_all | solution.py:528
  209.6 11.2 %copy-start.8 = (s32[384,2]{0,1:T(2,128)S(1)}, s32[384,2]{0,1:T(2,128)}, u32[]{:S(2)}) copy-start(s32[384,2]{0,1:T(2,128)} %param.9) | copy-start | bytes 9220
  220.8 12.1 %collective-permute-start.5 = (f32[2,3072]{1,0:T(2,128)}, f32[2,3072]{1,0:T(2,128)S(1)}, u32[]{:S(2)}, u32[]{:S(2)}) collective-permute-start(f32[2,3072]{1,0:T(2,128)} %get-tuple-element.56), channel_id=1, source_target_pairs={{0,1},{1,0},{2,3},{3,2},{4,5},{5,4},{6,7},{7,6},{8,9},{9,8},{10,11... | collective-permute-start | bytes 73736 | tf_op jit(solution)/shard_map/ppermute | solution.py:532
  224.1 8.9 %copy-start.9 = (f32[2,3072]{1,0:T(2,128)S(1)}, f32[2,3072]{1,0:T(2,128)}, u32[]{:S(2)}) copy-start(f32[2,3072]{1,0:T(2,128)} %get-tuple-element.56) | copy-start | bytes 73732
  239.4 1.3 copy-start

commit v3 on v2

--- a/solution.py
+++ b/solution.py
@@ -229,9 +229,9 @@
     up_pre = dot(rows, up_ref[...])
     sigma = jax.nn.sigmoid(gate_pre)
     active = gate_pre * sigma
-    active_ref[...] = active
+    active_ref[...] = active.astype(BF)
     hidden_ref[...] = (active * up_pre).astype(BF)
-    slope_ref[...] = up_pre * sigma * (1.0 + gate_pre * (1.0 - sigma))
+    slope_ref[...] = (up_pre * sigma * (1.0 + gate_pre * (1.0 - sigma))).astype(BF)
 
 
 def forward(core, own, other, gate_mat, up_mat):
@@ -245,8 +245,8 @@
         out_shape=[
             jax.ShapeDtypeStruct((1152, 2 * H), BF),
             jax.ShapeDtypeStruct((1152, Q), BF),
-            jax.ShapeDtypeStruct((1152, Q), F32),
-            jax.ShapeDtypeStruct((1152, Q), F32),
+            jax.ShapeDtypeStruct((1152, Q), BF),
+            jax.ShapeDtypeStruct((1152, Q), BF),
         ],
         name="forward",
     )(core, own, other, own, other, gate_mat, up_mat)
@@ -259,8 +259,8 @@
     grad = dot(rows_ref[...], down_ref[...])
     part = jnp.sum(hidden_ref[...].astype(F32) * grad, axis=1, keepdims=True)
     part_ref[...] = jnp.broadcast_to(part, (128, 128)).T[0:1, :]
-    gate = (grad * slope_ref[...]).astype(BF)
-    up = (grad * active_ref[...]).astype(BF)
+    gate = (grad * slope_ref[...].astype(F32)).astype(BF)
+    up = (grad * active_ref[...].astype(F32)).astype(BF)
     gate_ref[...] = gate
     up_ref[...] = up
     sent_ref[...] = dot(jnp.concatenate([gate, up], axis=1), back_ref[...]).astype(BF)
@@ -400,26 +400,29 @@
     ranks = ranks_ref[...]
     block = iota((TOK, F1), 1) % 8 // 2
     total = sum_ref[...] + dot(ones_where(ranks == column_slots(1)).astype(BF), flat_rows(two_ref))
-    hit = (ranks == column_slots(2)) & (block == b)
-    out_ref[...] = (total + dot(ones_where(hit).astype(BF), flat_rows(last_ref))).astype(BF)
+    last = flat_rows(last_ref)
+    for j in range(2):
+        hit = (ranks == column_slots(2)) & (block == 2 * b + j)
+        part = total[:, j * Q : (j + 1) * Q] + dot(ones_where(hit).astype(BF), last)
+        out_ref[:, j * Q : (j + 1) * Q] = part.astype(BF)
 
 
 def combine_two(ranks, lines, exp_t, gate_t, total, two):
     small = pl.BlockSpec((2, TOK), lambda b: (0, 0))
     return pl.pallas_call(
         combine_two_kernel,
-        grid=(4,),
+        grid=(2,),
         in_specs=[
             pl.BlockSpec((TOK, F1), lambda b: (0, 0)),
             small,
             small,
             small,
-            pl.BlockSpec((TOK, Q), lambda b: (0, b)),
-            pl.BlockSpec((E, 8, Q), lambda b: (0, 0, b)),
+            pl.BlockSpec((TOK, 2 * Q), lambda b: (0, b)),
+            pl.BlockSpec((E, 8, 2 * Q), lambda b: (0, 0, b)),
             pl.BlockSpec((E, 8, Q), lambda b: (0, 0, 4)),
             pl.BlockSpec((E, 8, 128), lambda b: (0, 0, 15)),
         ],
-        out_specs=[pl.BlockSpec((TOK, Q), lambda b: (0, b)), small],
+        out_specs=[pl.BlockSpec((TOK, 2 * Q), lambda b: (0, b)), small],
         out_shape=[jax.ShapeDtypeStruct((TOK, H), BF), jax.ShapeDtypeStruct((2, TOK), F32)],
         name="combine_two",
     )(ranks, lines, exp_t, gate_t, total, two, two, two)

time: 248 us -> 247 us (level)
  no operation moved by 1% of the time
where the time goes in v3:
time: 247 us; the launch traced here: 246 us
  blocking collectives  109 us (44%)
  Pallas kernels  93.2 us (38%)
  waiting for transfers between devices  17.2 us (7%)
  starting transfers between devices  12.2 us (5%)
  matrix products  5.73 us (2%)
  local copies, waits for them, and re-layouts  4.61 us (2%)
  other arithmetic  2.95 us (1%)
    all_to_all x2, blocking collectives, to_experts(): return lax.all_to_all(x, 'ep', split_axis=0, concat_axis=0, tiled=True)  109 us
    pallas_call x2, Pallas kernels, middle(): pl.pallas_call(middle_kernel, grid=(steps,), in_specs=packed_specs(0, 1,...  18.6 us
    all_to_all x2, waiting for transfers between devices, to_experts(): return lax.all_to_all(x, 'ep', split_axis=0, concat_axis=0, tiled=True)  17.2 us
    pallas_call x1, Pallas kernels, forward(): pl.pallas_call(forward_kernel, grid=(9,), in_specs=packed_specs(1, 2, 12)...  15.3 us
    pallas_call x1, Pallas kernels, weight_grads(): pl.pallas_call(weight_grads_kernel, grid=(6,), in_specs=[pl.BlockSpec((11...  11.2 us
    all_to_all x2, starting transfers between devices, to_experts(): return lax.all_to_all(x, 'ep', split_axis=0, concat_axis=0, tiled=True)  11.2 us
    pallas_call x1, Pallas kernels, down_grads(): pl.pallas_call(down_grads_kernel, grid=(6,), in_specs=[pl.BlockSpec((1152...  8.86 us
    pallas_call x1, Pallas kernels, send_first(): pl.pallas_call(send_first_kernel, grid=(3,), in_specs=[small, small, sour...  7.95 us
  transfers between devices with their start and end apart: 8, of which 2 were waited for; matrix products, arithmetic and copies ran while one was open for 4% of the time, Pallas kernels for 30%

profile of v3, /device:TPU:0, one launch (start us, length us, event | category | flops | bytes accessed | tf_op | source)
XLA Modules:
  0.0 246.0 jit_solution(3679820618129023257)
XLA Ops:
  0.6 7.9 %send_first.1 = (bf16[64,8,4992]{2,1,0:T(8,128)(2,1)}, f32[512,384]{1,0:T(8,128)}, f32[512,384]{1,0:T(8,128)}, f32[2,384]{1,0:T(2,128)}) custom-call(s32[2,384]{1,0:T(2,128)} %bitcast.31, f32[2,384]{1,0:T(2,128)} %bitcast.33, bf16[384,1536]{1,0:T(8,128)(2,1)} %tok_ref.1, bf16[384,1536]{1,0:T(8,128)(2,1)} %src_ref.1), custom_call_target="tpu_custom_call" | custom-call | tf_op jit(solution)/shard_map/send_first/pallas_call | solution.py:127
  8.6 74.1 %all_to_all.20.own_ref.own_last_ref.refs_0_ = bf16[64,8,4992]{2,1,0:T(8,128)(2,1)} all-to-all(bf16[64,8,4992]{2,1,0:T(8,128)(2,1)} %get-tuple-element.34), channel_id=1, replica_groups=mesh['ep'=64,'tp'=2] {'ep'}, dimensions={0} | all-to-all | bytes 10223616 | tf_op jit(solution)/shard_map/all_to_all | solution.py:531
  82.7 0.0 collective-permute-start
  82.7 6.0 %send.1 = bf16[64,8,1920]{2,1,0:T(8,128)(2,1)} custom-call(f32[512,384]{1,0:T(8,128)} %get-tuple-element.41.ranks_ref, f32[512,384]{1,0:T(8,128)} %get-tuple-element.42.gates_ref, bf16[384,1536]{1,0:T(8,128)(2,1)} %src_ref.1), custom_call_target="tpu_custom_call" | custom-call | tf_op jit(solution)/shard_map/send/pallas_call | solution.py:171
  88.6 35.2 %all_to_all.21.refs_0_.refs_2_ = bf16[64,8,1920]{2,1,0:T(8,128)(2,1)} all-to-all(bf16[64,8,1920]{2,1,0:T(8,128)(2,1)} %send.1), channel_id=1, replica_groups=mesh['ep'=64,'tp'=2] {'ep'}, dimensions={0} | all-to-all | bytes 3932160 | tf_op jit(solution)/shard_map/all_to_all | solution.py:531
  123.8 0.0 collective-permute-start.2
  123.8 5.3 %turn.1.refs_2_.refs_4_ = bf16[3072,384]{1,0:T(8,128)(2,1)} custom-call(bf16[384,3072]{1,0:T(8,128)(2,1)} %bitcast.30), custom_call_target="tpu_custom_call" | custom-call | tf_op jit(solution)/shard_map/turn/pallas_call | solution.py:469
  129.1 4.2 %turn_back.1.refs_3_.refs_5_ = bf16[768,1536]{1,0:T(8,128)(2,1)} custom-call(s32[1]{0:T(128)} %bitcast.2.core_ref, bf16[3072,384]{1,0:T(8,128)(2,1)} %bitcast.28, bf16[3072,384]{1,0:T(8,128)(2,1)} %bitcast.26), custom_call_target="tpu_custom_call" | custom-call | tf_op jit(solution)/shard_map/turn_back/pallas_call | solution.py:486
  133.3 0.0 collective-permute-done.other_ref.other_last_ref.refs_1_
  133.3 15.3 %forward.1 = (bf16[1152,3072]{1,0:T(8,128)(2,1)}, bf16[1152,384]{1,0:T(8,128)(2,1)}, bf16[1152,384]{1,0:T(8,128)(2,1)}, bf16[1152,384]{1,0:T(8,128)(2,1)}) custom-call(s32[1]{0:T(128)} %bitcast.2.core_ref, bf16[64,8,4992]{2,1,0:T(8,128)(2,1)} %all_to_all.20.own_ref.own_last_ref.refs_0_, ...), custom_call_target="tpu_custom_call" | custom-call | tf_op jit(solution)/shard_map/forward/pallas_call | solution.py:240
  148.6 8.2 %middle.2 = (bf16[512,3072]{1,0:T(8,128)(2,1)}, bf16[512,384]{1,0:T(8,128)(2,1)}, bf16[512,384]{1,0:T(8,128)(2,1)}, f32[1,512]{1,0:T(1,128)}, bf16[512,1536]{1,0:T(8,128)(2,1)}) custom-call(s32[1]{0:T(128)} %bitcast.2.core_ref, bf16[64,8,4992]{2,1,0:T(8,128)(2,1)} %all_to_all.20.own_ref.own_last_ref.refs_0_, ...), custom_call_target="tpu_custom_call" | custom-call | tf_op jit(solution)/shard_map/middle/pallas_call | solution.py:275
  156.9 0.6 collective-permute-start.1
  157.5 0.0 copy-start.1
  157.5 0.0 collective-permute-done.2.refs_1_.refs_3_
  157.5 10.4 %middle.3 = (bf16[640,3072]{1,0:T(8,128)(2,1)}, bf16[640,384]{1,0:T(8,128)(2,1)}, bf16[640,384]{1,0:T(8,128)(2,1)}, f32[1,640]{1,0:T(1,128)}, bf16[640,1536]{1,0:T(8,128)(2,1)}) custom-call(s32[1]{0:T(128)} %bitcast.2.core_ref, bf16[64,8,1920]{2,1,0:T(8,128)(2,1)} %all_to_all.21.refs_0_.refs_2_, bf16[64,8,1920]{2,1,0:T(8,128)(2,1)} %collective-permute-done.2.refs_1_.refs_3_, ...), custom_call_target="tpu_custom_call" | custom-call | tf_op jit(solution)/shard_map/middle/pallas_call | solution.py:275
  167.9 0.1 collective-permute-start.3
  168.0 0.0 copy-done.1
  168.0 0.0 copy-done.5
  168.0 0.0 copy-start.2
  168.0 0.0 copy-start.7
  168.0 1.0 fusion.4
  169.1 0.6 copy-done.2
  169.7 0.0 copy-done.7
  169.7 1.0 fusion
  170.7 0.0 collective-permute-done.1
  170.8 2.9 %fusion.1 = bf16[64,8,1536]{2,1,0:T(8,128)(2,1)} fusion(bf16[512,1536]{1,0:T(8,128)(2,1)} %collective-permute-done.1, bf16[512,1536]{1,0:T(8,128)(2,1)S(1)} %fusion), kind=kLoop, calls=%fused_computation.4 | loop fusion | flops 3145728 | bytes 4718592 | tf_op jit(solution)/shard_map/reshape | solution.py:567
  173.7 0.0 copy-start.13
  173.7 0.0 copy-start.12
  173.7 0.0 copy-start.4
  173.7 5.9 %all-to-all-start.1 = ((bf16[64,8,1536]{2,1,0:T(8,128)(2,1)}), bf16[64,8,1536]{2,1,0:T(8,128)(2,1)}, u32[]{:S(2)}, u32[]{:S(2)}) async-start(bf16[64,8,1536]{2,1,0:T(8,128)(2,1)} %fusion.1), calls=%async_computation.1 | async-start | bytes 3145728 | tf_op jit(solution)/shard_map/all_to_all | solution.py:531
  179.6 0.0 copy-done.13
  179.6 0.0 copy-done.12
  179.6 0.0 copy-start.10
  179.7 0.3 collective-permute-start.4
  179.9 0.0 copy-done.4
  179.9 0.0 copy-start.3
  179.9 0.0 copy-start.6
  179.9 1.2 fusion.2
  181.1 0.0 copy-done.10
  181.2 0.4 copy-done.3
  181.6 0.1 copy-done.6
  181.7 2.5 %add_convert_fusion.mine_ref.mine_last_ref = bf16[640,1536]{1,0:T(8,128)(2,1)} fusion(f32[640,1536]{1,0:T(8,128)S(1)} %fusion.2, bf16[640,384]{1,0:T(8,128)(2,1)S(1)} %copy-done.6, bf16[1,3072,384]{2,1,0:T(8,128)(2,1)S(1)} %copy-done.3, s32[]{:T(128)S(6)} %select_n.4), kind=kOutput, calls=%fused_computation | convolution fusion | flops 756940800 | bytes 7569412 | tf_op jit(solution)/shard_map/dot_general | solution.py:29
  184.2 0.0 collective-permute-done.4.got_part_ref
  184.2 0.0 copy-start.11
  184.2 0.0 collective-permute-done.3.got_ref.got_last_ref
  184.2 0.6 copy-done.11
  184.8 5.0 %pack.1 = bf16[64,8,2048]{2,1,0:T(8,128)(2,1)} custom-call(bf16[640,1536]{1,0:T(8,128)(2,1)} %add_convert_fusion.mine_ref.mine_last_ref, bf16[640,1536]{1,0:T(8,128)(2,1)} %collective-permute-done.3.got_ref.got_last_ref, bf16[640,1536]{1,0:T(8,128)(2,1)} %add_convert_fusion.mine_ref.mine_last_ref, ...), custom_call_target="tpu_custom_call" | custom-call | tf_op jit(solution)/shard_map/pack/pallas_call | solution.py:331
  189.8 14.7 %all-to-all-done.1.one_ref = bf16[64,8,1536]{2,1,0:T(8,128)(2,1)} async-done(((bf16[64,8,1536]{2,1,0:T(8,128)(2,1)}), bf16[64,8,1536]{2,1,0:T(8,128)(2,1)}, u32[]{:S(2)}, u32[]{:S(2)}) %all-to-all-start.1) | async-done | bytes 1572896 | tf_op jit(solution)/shard_map/all_to_all | solution.py:531
  204.5 5.3 %all-to-all-start.3 = ((bf16[64,8,2048]{2,1,0:T(8,128)(2,1)}), bf16[64,8,2048]{2,1,0:T(8,128)(2,1)S(1)}, u32[]{:S(2)}, u32[]{:S(2)}) async-start(bf16[64,8,2048]{2,1,0:T(8,128)(2,1)} %pack.1), calls=%async_computation.3 | async-start | bytes 4194304 | tf_op jit(solution)/shard_map/all_to_all | solution.py:531
  209.8 0.0 copy-start.8
  209.8 11.2 %weight_grads.1 = (bf16[3072,384]{1,0:T(8,128)(2,1)}, bf16[3072,384]{1,0:T(8,128)(2,1)}, f32[2,3072]{1,0:T(2,128)}) custom-call(bf16[1152,3072]{1,0:T(8,128)(2,1)} %get-tuple-element.50.x_ref, bf16[512,384]{1,0:T(8,128)(2,1)} %get-tuple-element.38.g1_ref, bf16[512,384]{1,0:T(8,128)(2,1)} %get-tuple-element.39.u1_ref, ...), custom_call_target="tpu_custom_call" | custom-call | tf_op jit(solution)/shard_map/weight_grads/pallas_call | solution.py:519
  221.1 0.0 collective-permute-start.5
  221.1 0.0 copy-done.8
  221.1 0.8 copy.15.exp_ref
  221.9 2.4 token_ranks.1.ranks_ref
  224.3 0.0 copy-start.9
  224.3 8.9 %down_grads.1 = (bf16[384,3072]{1,0:T(8,128)(2,1)}, f32[1,384]{1,0:T(1,128)}) custom-call(bf16[1152,384]{1,0:T(8,128)(2,1)} %get-tuple-element.35.refs_4_.refs_6_.hidden_ref, bf16[512,3072]{1,0:T(8,128)(2,1)} %get-tuple-element.53.one_ref, bf16[640,3072]{1,0:T(8,128)(2,1)} %get-tuple-element.54.two_ref), custom_call_target="tpu_custom_call" | custom-call | tf_op jit(solution)/shard_map/down_grads/pallas_call | solution.py:449
  233.2 0.0 collective-permute-done.5
  233.2 0.0 copy-done.9
  233.2 0.6 fusion.16
  233.8 3.4 %combine_one.1.refs_0_ = f32[384,1536]{1,0:T(8,128)} custom-call(f32[384,512]{1,0:T(8,128)} %token_ranks.1.ranks_ref, bf16[64,8,1536]{2,1,0:T(8,128)(2,1)} %all-to-all-done.1.one_ref), custom_call_target="tpu_custom_call" | custom-call | tf_op jit(solution)/shard_map/combine_one/pallas_call | solution.py:372
  237.2 2.4 all-to-all-done.3.refs_1_.refs_2_.refs_3_
  239.7 1.3 copy-done
  241.0 4.9 %combine_two.1 = (bf16[384,1536]{1,0:T(8,128)(2,1)}, f32[2,384]{1,0:T(2,128)}) custom-call(f32[384,512]{1,0:T(8,128)} %token_ranks.1.ranks_ref, f32[2,384]{1,0:T(2,128)} %get-tuple-element.33.line_ref, s32[2,384]{1,0:T(2,128)} %bitcast.32, f32[2,384]{1,0:T(2,128)} %bitcast.34, f32[384,1536]{1,0:T(8,128)} %combine_one.1.refs_0_, ...), custom_call_target="tpu_custom_call" | custom-call | tf_op jit(solution)/shard_map/combine_two/pallas_call | solution.py:412
  (5 shorter events, 0.0 us)
Async XLA Ops:
  82.7 50.6 %collective-permute-start = (bf16[64,8,4992]{2,1,0:T(8,128)(2,1)}, bf16[64,8,4992]{2,1,0:T(8,128)(2,1)}, u32[]{:S(2)}, u32[]{:S(2)}) collective-permute-start(bf16[64,8,4992]{2,1,0:T(8,128)(2,1)} %all_to_all.20.own_ref.own_last_ref.refs_0_), channel_id=1, source_target_pairs={{0,1},{1,0},{2,3},{3,2},{4,5},{5,4},{6,7},{7,6},{8,9},{9,8},{10,11... | collective-permute-start | bytes 15335432 | tf_op jit(solution)/shard_map/ppermute | solution.py:535
  123.8 33.7 %collective-permute-start.2 = (bf16[64,8,1920]{2,1,0:T(8,128)(2,1)}, bf16[64,8,1920]{2,1,0:T(8,128)(2,1)}, u32[]{:S(2)}, u32[]{:S(2)}) collective-permute-start(bf16[64,8,1920]{2,1,0:T(8,128)(2,1)} %all_to_all.21.refs_0_.refs_2_), channel_id=1, source_target_pairs={{0,1},{1,0},{2,3},{3,2},{4,5},{5,4},{6,7},{7,6},{8,9},{9,8},{10,11... | collective-permute-start | bytes 5898248 | tf_op jit(solution)/shard_map/ppermute | solution.py:535
  156.9 13.9 %collective-permute-start.1 = (bf16[512,1536]{1,0:T(8,128)(2,1)}, bf16[512,1536]{1,0:T(8,128)(2,1)}, u32[]{:S(2)}, u32[]{:S(2)}) collective-permute-start(bf16[512,1536]{1,0:T(8,128)(2,1)} %get-tuple-element.40), channel_id=1, source_target_pairs={{0,1},{1,0},{2,3},{3,2},{4,5},{5,4},{6,7},{7,6},{8,9},{9,8},{10,11... | collective-permute-start | bytes 4718600 | tf_op jit(solution)/shard_map/ppermute | solution.py:535
  157.5 10.5 %copy-start.1 = (bf16[1,3072,384]{2,1,0:T(8,128)(2,1)S(1)}, bf16[1,3072,384]{2,1,0:T(8,128)(2,1)}, u32[]{:S(2)}) copy-start(bf16[1,3072,384]{2,1,0:T(8,128)(2,1)} %param.12) | copy-start | bytes 7077892
  157.5 10.5 %copy-start.5 = (bf16[512,384]{1,0:T(8,128)(2,1)S(1)}, bf16[512,384]{1,0:T(8,128)(2,1)}, u32[]{:S(2)}) copy-start(bf16[512,384]{1,0:T(8,128)(2,1)} %get-tuple-element.39.u1_ref) | copy-start | bytes 1179652
  167.9 16.2 %collective-permute-start.3 = (bf16[640,1536]{1,0:T(8,128)(2,1)}, bf16[640,1536]{1,0:T(8,128)(2,1)}, u32[]{:S(2)}, u32[]{:S(2)}) collective-permute-start(bf16[640,1536]{1,0:T(8,128)(2,1)} %get-tuple-element.45), channel_id=1, source_target_pairs={{0,1},{1,0},{2,3},{3,2},{4,5},{5,4},{6,7},{7,6},{8,9},{9,8},{10,11... | collective-permute-start | bytes 5898248 | tf_op jit(solution)/shard_map/ppermute | solution.py:535
  168.0 1.7 copy-start.2
  168.0 1.7 copy-start.7
  173.7 5.9 %copy-start.13 = (f32[1,512]{1,0:T(1,128)S(1)}, f32[1,512]{1,0:T(1,128)}, u32[]{:S(2)}) copy-start(f32[1,512]{1,0:T(1,128)} %get-tuple-element.46) | copy-start | bytes 6148
  173.7 5.9 %copy-start.12 = (f32[1,640]{1,0:T(1,128)S(1)}, f32[1,640]{1,0:T(1,128)}, u32[]{:S(2)}) copy-start(f32[1,640]{1,0:T(1,128)} %get-tuple-element.47) | copy-start | bytes 7684
  173.7 6.2 %copy-start.4 = (bf16[640,384]{1,0:T(8,128)(2,1)S(1)}, bf16[640,384]{1,0:T(8,128)(2,1)}, u32[]{:S(2)}) copy-start(bf16[640,384]{1,0:T(8,128)(2,1)} %get-tuple-element.44.u2_ref) | copy-start | bytes 1474564
  173.7 30.8 %all-to-all-start.1 = ((bf16[64,8,1536]{2,1,0:T(8,128)(2,1)}), bf16[64,8,1536]{2,1,0:T(8,128)(2,1)}, u32[]{:S(2)}, u32[]{:S(2)}) async-start(bf16[64,8,1536]{2,1,0:T(8,128)(2,1)} %fusion.1), calls=%async_computation.1 | async-start | bytes 3145728 | tf_op jit(solution)/shard_map/all_to_all | solution.py:531
  179.6 1.5 copy-start.10
  179.7 4.5 %collective-permute-start.4 = (f32[1,1152]{1,0:T(1,128)S(1)}, f32[1,1152]{1,0:T(1,128)S(1)}, u32[]{:S(2)}, u32[]{:S(2)}) collective-permute-start(f32[1,1152]{1,0:T(1,128)S(1)} %constant_dynamic-update-slice_fusion.part_ref), channel_id=1, source_target_pairs={{0,1},{1,0},{2,3},{3,2},{4,5},{5,4},{6,7},{7,6},{8,9},{9,8},{10,11... | collective-permute-start | bytes 13832 | tf_op jit(solution)/shard_map/ppermute | solution.py:535
  179.9 1.7 copy-start.3
  179.9 1.7 copy-start.6
  184.2 0.6 copy-start.11
  204.5 35.2 %all-to-all-start.3 = ((bf16[64,8,2048]{2,1,0:T(8,128)(2,1)}), bf16[64,8,2048]{2,1,0:T(8,128)(2,1)S(1)}, u32[]{:S(2)}, u32[]{:S(2)}) async-start(bf16[64,8,2048]{2,1,0:T(8,128)(2,1)} %pack.1), calls=%async_computation.3 | async-start | bytes 4194304 | tf_op jit(solution)/shard_map/all_to_all | solution.py:531
  209.8 11.2 %copy-start.8 = (s32[384,2]{0,1:T(2,128)S(1)}, s32[384,2]{0,1:T(2,128)}, u32[]{:S(2)}) copy-start(s32[384,2]{0,1:T(2,128)} %param.9) | copy-start | bytes 9220
  221.1 12.1 %collective-permute-start.5 = (f32[2,3072]{1,0:T(2,128)}, f32[2,3072]{1,0:T(2,128)S(1)}, u32[]{:S(2)}, u32[]{:S(2)}) collective-permute-start(f32[2,3072]{1,0:T(2,128)} %get-tuple-element.56), channel_id=1, source_target_pairs={{0,1},{1,0},{2,3},{3,2},{4,5},{5,4},{6,7},{7,6},{8,9},{9,8},{10,11... | collective-permute-start | bytes 73736 | tf_op jit(solution)/shard_map/ppermute | solution.py:535
  224.3 8.9 %copy-start.9 = (f32[2,3072]{1,0:T(2,128)S(1)}, f32[2,3072]{1,0:T(2,128)}, u32[]{:S(2)}) copy-start(f32[2,3072]{1,0:T(2,128)} %get-tuple-element.56) | copy-start | bytes 73732
  239.7 1.3 copy-start
